TPU v7x, 32 devices: a whole 2x2x4 slice. The times are simulated.
32 devices in a mesh: sp: 8 (over z, core), tp: 4 (over y, x).
Axes of the slice: x: 2, y: 2, z: 4, core: 2. Of those that a mesh axis runs over, the one named last changes fastest.
Arguments:
- moe_input: bfloat16 [1024, 2048], P('sp', 'tp'), may hold values from -6 to 6
- cotangent: bfloat16 [1024, 2048], P('sp', 'tp'), may hold values from -6 to 6
- routes: int32 [1024, 2], P('sp'), may hold values from 0 to 7, all different within a row; in each aligned block of 128 rows (0 to 127, 128 to 255, ...) at most 40 rows name the same one
- route_weights: float32 [1024, 2], P('sp'), may hold values from 0.2 to 1
- gate_branch: bfloat16 [1024, 2560], P('sp', 'tp'), may hold values from -6 to 6
- log_decay: float32 [1024, 2560], P('sp', 'tp'), may hold values from -0.12 to 0
- states: float32 [1024, 2560], P('sp', 'tp'), may hold values from -6 to 6
- w_gate: bfloat16 [8, 2048, 2048], P('sp', None, 'tp'), may hold values from -0.125 to 0.125
- w_up: bfloat16 [8, 2048, 2048], P('sp', None, 'tp'), may hold values from -0.125 to 0.125
- w_down: bfloat16 [8, 2048, 2048], P('sp', 'tp'), may hold values from -0.125 to 0.125
- out_proj: bfloat16 [2048, 2560], P('sp', 'tp'), may hold values from -0.125 to 0.125
Outputs:
- grad_w_gate: float32 [8, 2048, 2048], P('sp', None, 'tp')
- grad_w_up: float32 [8, 2048, 2048], P('sp', None, 'tp')
- grad_w_down: float32 [8, 2048, 2048], P('sp', 'tp')
- grad_out_proj: float32 [2048, 2560], P('sp', 'tp')
- grad_gate_branch: bfloat16 [1024, 2560], P('sp', 'tp')
- grad_log_decay: bfloat16 [1024, 2560], P('sp', 'tp')
- grad_input_term: float32 [1024, 2560], P('sp', 'tp')
Inputs may be any that keep to these rules, and one draw needn't show every extreme that they name: `routes`: in the rows of one device no expert is named by more than 40 entries, and in every draw some expert is named by exactly 40 entries of one device's rows.
All inputs are finite; a program needn't handle non-finite values.
Results may differ from a plain program's by a relative error of at most 0.025.
Values may be sent and summed in bfloat16 or wider, within the bound.
A program may use at most 64 MiB of HBM per device.

v0:
```python
import jax
import jax.numpy as jnp
from jax import lax
from jax.experimental import pallas as pl
from jax.experimental.pallas import tpu as pltpu
from jax.sharding import PartitionSpec as P

BF = jnp.bfloat16
F32 = jnp.float32
CORES = 2
GELU_C = 0.7978845608028654
GELU_A = 0.044715


def silu_parts(pre_gate):
    sigmoid_val = jax.nn.sigmoid(pre_gate)
    return (pre_gate * sigmoid_val, sigmoid_val * (1.0 + pre_gate * (1.0 - sigmoid_val)))


def contract_rows(left_mat, right_mat):
    return lax.dot_general(
        left_mat, right_mat, (((0,), (0,)), ((), ())), preferred_element_type=F32
    )


def contract_cols(left_mat, right_mat):
    return lax.dot_general(
        left_mat, right_mat, (((1,), (1,)), ((), ())), preferred_element_type=F32
    )


def gelu_parts(x):
    t = jnp.tanh(GELU_C * (x + GELU_A * (x * x * x)))
    half = 0.5 * (1.0 + t)
    slope = half + 0.5 * x * (1.0 - t * t) * (GELU_C * (1.0 + 3.0 * GELU_A * x * x))
    return x * half, slope


def selection(routes_t, weights_t, groups, room):
    picks, toks = routes_t.shape
    experts = lax.broadcasted_iota(jnp.int32, (groups, toks), 0)
    named = jnp.zeros((groups, toks), F32)
    weight = jnp.zeros((groups, toks), F32)
    for k in range(picks):
        hit = routes_t[k : k + 1, :] == experts
        named = named + jnp.where(hit, 1.0, 0.0)
        weight = weight + jnp.where(hit, weights_t[k : k + 1, :], 0.0)
    rows = lax.broadcasted_iota(jnp.int32, (toks, toks), 0)
    cols = lax.broadcasted_iota(jnp.int32, (toks, toks), 1)
    before = jnp.where(rows < cols, 1.0, 0.0).astype(BF)
    slot = jnp.dot(named.astype(BF), before, preferred_element_type=F32)
    slot = jnp.where(named > 0.5, slot, -1.0)
    place = lax.broadcasted_iota(jnp.int32, (room, toks), 0).astype(F32)
    picked, column = [], []
    for e in range(groups):
        one = jnp.where(slot[e : e + 1, :] == place, 1.0, 0.0)
        picked.append(one)
        column.append(jnp.sum(one * weight[e : e + 1, :], axis=1, keepdims=True))
    return jnp.concatenate(picked, axis=0).astype(BF), jnp.concatenate(column, axis=0)


def greet(groups, parts, mine, col):
    barrier = pltpu.get_barrier_semaphore()
    for d in range(1, groups):
        pl.semaphore_signal(
            barrier, inc=1, device_id={"sp": lax.rem(mine + d, groups)},
            device_id_type=pl.DeviceIdType.MESH,
        )
    for d in range(1, parts):
        pl.semaphore_signal(
            barrier, inc=1, device_id={"tp": lax.rem(col + d, parts)},
            device_id_type=pl.DeviceIdType.MESH,
        )
    pl.semaphore_wait(barrier, groups + parts - 2)


def remote(src, dst, send, recv, axis, peer):
    return pltpu.make_async_remote_copy(
        src_ref=src, dst_ref=dst, send_sem=send, recv_sem=recv,
        device_id={axis: peer}, device_id_type=pl.DeviceIdType.MESH,
    )


def whole_kernel(
    groups, parts, room, chunked,
    routes_ref, weights_ref, x_any, cot_any, gate_any, states_any, decay_any, proj_any,
    wg_any, wu_any, wd_any,
    gg_ref, gu_ref, gd_ref, outp_ref, ggate_ref, gdecay_ref, gin_ref,
    x_ref, cot_ref, gate_ref, states_ref, decay_ref, wg, wu, wd,
    out_x, out_c, rows_x, rows_c, proj_all, mixed_all, mix_own, gg, gu, gd,
    terms, shares, summed, back, flipped, blocks, carry_own, carry_in, prev_in,
    a_send, a_recv, t_send, t_recv, z_send, z_recv, c_send, c_recv,
    s_send, s_recv, r_send, r_recv, g_send, g_recv, b_send, b_recv, k_send, k_recv, p_send, p_recv,
    l_sem, w_sem,
):
    mine, col = lax.axis_index("sp"), lax.axis_index("tp")
    toks, width = x_ref.shape
    model = rows_x.shape[2]
    depth = groups // CORES
    z, core = mine // CORES, lax.rem(mine, CORES)
    size = groups * room

    def near(width_of, index):
        return pl.ds(pl.multiple_of(index * width_of, width_of), width_of)

    loads = []
    for i, (s, t) in enumerate((
        (x_any, x_ref), (cot_any, cot_ref), (gate_any, gate_ref), (states_any, states_ref),
        (proj_any, proj_all.at[mine]), (decay_any, decay_ref),
        (wg_any.at[0], wg), (wu_any.at[0], wu), (wd_any.at[0], wd),
    )):
        o = pltpu.make_async_copy(s, t, l_sem.at[i])
        o.start()
        loads.append(o)

    picked, weight = selection(routes_ref[...], weights_ref[...], groups, room)
    loads[0].wait()
    got = jnp.dot(picked, x_ref[...], preferred_element_type=F32).astype(BF)
    for e in range(groups):
        out_x[e] = got[e * room : (e + 1) * room]
    loads[1].wait()
    got_c = jnp.dot(picked, cot_ref[...], preferred_element_type=F32)
    got_c = (got_c * weight).astype(BF)
    for e in range(groups):
        out_c[e] = got_c[e * room : (e + 1) * room]
    greet(groups, parts, mine, col)

    here = near(width, col)
    sends, own = [], []
    arrivals = [[None] * groups for _ in range(2)]
    for a, (src, dst) in enumerate(((out_x, rows_x), (out_c, rows_c))):
        for d in range(1, groups):
            peer = lax.rem(mine + d, groups)
            c = remote(src.at[peer], dst.at[mine, :, here], a_send.at[a, d], a_recv.at[a, d], "sp", peer)
            c.start()
            arrivals[a][d] = c
            sends.append(c)
        o = pltpu.make_async_copy(src.at[mine], dst.at[mine, :, here], w_sem.at[a])
        o.start()
        own.append(o)

    pairs = (proj_all, mixed_all)

    def chain(a, step, wait=False):
        buf = pairs[a]
        right = buf.at[jnp.maximum(z - step, 0) * CORES + core]
        left = buf.at[jnp.minimum(z + step, depth - 1) * CORES + core]
        up = jnp.minimum(z + 1, depth - 1) * CORES + core
        down = jnp.maximum(z - 1, 0) * CORES + core
        for way, ref, peer, ok in (
            (0, right, up, jnp.logical_and(z - step >= 0, z + 1 < depth)),
            (1, left, down, jnp.logical_and(z + step < depth, z >= 1)),
        ):
            @pl.when(ok)
            def _(way=way, ref=ref, peer=peer):
                c = remote(ref, ref, z_send.at[a, way, step], z_recv.at[a, way, step], "sp", peer)
                c.wait_send() if wait else c.start()

    partner = z * CORES + (1 - core)

    def across(a, step, way, mode):
        ok = z - step >= 0 if way == 0 else z + step < depth
        zz = jnp.maximum(z - step, 0) if way == 0 else jnp.minimum(z + step, depth - 1)
        ref = pairs[a].at[zz * CORES + (1 - core if mode == "recv" else core)]

        @pl.when(ok)
        def _():
            c = remote(ref, ref, c_send.at[a, way, step], c_recv.at[a, way, step], "sp", partner)
            if mode == "start":
                c.start()
            elif mode == "send":
                c.wait_send()
            else:
                c.wait_recv()

    def advance(a, step):
        buf = pairs[a]
        from_l = buf.at[jnp.maximum(z - 1 - step, 0) * CORES + core]
        from_r = buf.at[jnp.minimum(z + 1 + step, depth - 1) * CORES + core]
        for way, ok, ref in ((0, z - 1 - step >= 0, from_l), (1, z + 1 + step < depth, from_r)):
            @pl.when(ok)
            def _(way=way, ref=ref):
                remote(ref, ref, z_send.at[a, way, step], z_recv.at[a, way, step],
                       "sp", lax.rem(mine + 1, groups)).wait_recv()
        if step + 1 < depth - 1:
            chain(a, step + 1)
        across(a, step + 1, 0, "start")
        across(a, step + 1, 1, "start")

    def settle(a):
        for step in range(depth - 1):
            chain(a, step, True)
        for step in range(depth):
            for way in range(2):
                if step or not way:
                    across(a, step, way, "send")

    def collected(a):
        for step in range(depth):
            for way in range(2):
                if step or not way:
                    across(a, step, way, "recv")

    loads[4].wait()
    chain(0, 0)
    across(0, 0, 0, "start")

    gathers = [[], []]

    def gather(a, src, dst):
        if chunked:
            for d in range(groups):
                at = lax.rem(mine + groups - d, groups)
                if d:
                    arrivals[a][d].wait_recv()
                for p in range(1, parts):
                    c = remote(dst.at[at, :, here] if d else src.at[mine], dst.at[at, :, here],
                               t_send.at[a, d, p], t_recv.at[a, d, p], "tp", lax.rem(col + p, parts))
                    c.start()
                    gathers[a].append(c)
            own[a].wait()
        else:
            own[a].wait()
            for d in range(1, groups):
                arrivals[a][d].wait_recv()
            for p in range(1, parts):
                c = remote(dst.at[:, :, here], dst.at[:, :, here],
                           t_send.at[a, 0, p], t_recv.at[a, 0, p], "tp", lax.rem(col + p, parts))
                c.start()
                gathers[a].append(c)
        sends.extend(gathers[a])

    gather(0, out_x, rows_x)
    loads[2].wait()
    loads[3].wait()
    act, branch_slope = gelu_parts(gate_ref[...].astype(F32))
    mix_own[...] = (act * states_ref[...]).astype(BF)
    gather(1, out_c, rows_c)
    o = pltpu.make_async_copy(mix_own, mixed_all.at[mine], w_sem.at[3])
    o.start()
    o.wait()
    for i in range(6, 9):
        loads[i].wait()
    for c in gathers[0]:
        c.wait_recv()
    row_data = rows_x[...].reshape(size, model)
    pre_gate = jnp.dot(row_data, wg[...], preferred_element_type=F32)
    pre_up = jnp.dot(row_data, wu[...], preferred_element_type=F32)
    active, slope = silu_parts(pre_gate)
    hidden = (active * pre_up).astype(BF)
    lean = pre_up * slope
    advance(0, 0)
    if depth > 2:
        advance(0, 1)
    for c in gathers[1]:
        c.wait_recv()
    grad_hidden = contract_cols(rows_c[...].reshape(size, model), wd[...])
    grad_pre_gate = (grad_hidden * lean).astype(BF)
    grad_pre_up = (grad_hidden * active).astype(BF)
    for d in list(range(1, parts)) + [0]:
        part = near(width, lax.rem(col + d, parts))
        term = contract_cols(grad_pre_gate, wg[part, :]) + contract_cols(grad_pre_up, wu[part, :])
        terms[d] = term.astype(BF).reshape(groups, room, width)

    share_copies = {}
    order = list(range(1, groups)) + [0]
    for d in order if chunked else [0]:
        at = lax.rem(mine + d, groups)
        for p in range(1, parts):
            src = terms.at[p, at] if chunked else terms.at[p]
            dst = shares.at[p - 1, at] if chunked else shares.at[p - 1]
            c = remote(src, dst, s_send.at[d, p], s_recv.at[d, p], "tp", lax.rem(col + p, parts))
            c.start()
            share_copies[d, p] = c
            sends.append(c)
    for step in range(2, depth - 1):
        advance(0, step)
    chain(1, 0)
    across(1, 0, 0, "start")

    stores = []

    def piece(kind, p):
        part = slice(p * width, (p + 1) * width)
        if kind == 2:
            gd[:, part] = contract_rows(hidden, rows_c[:, :, part].reshape(size, width)).astype(BF)
            s, t = gd.at[:, part], gd_ref.at[:, part]
        else:
            grad, buf, out = ((grad_pre_gate, gg, gg_ref), (grad_pre_up, gu, gu_ref))[kind]
            buf[part, :] = contract_rows(rows_x[:, :, part].reshape(size, width), grad).astype(BF)
            s, t = buf.at[part], out.at[part]
        o = pltpu.make_async_copy(s, t, w_sem.at[4 + kind * parts + p])
        o.start()
        stores.append(o)

    pieces = [(kind, p) for kind in range(3) for p in range(parts)]
    back_copies = []
    for d in order:
        if pieces:
            piece(*pieces.pop(0))
        at = lax.rem(mine + d, groups)
        if chunked or d == 1:
            for p in range(1, parts):
                share_copies[d if chunked else 0, p].wait_recv()
        total = terms[0, at].astype(F32)
        for p in range(1, parts):
            total = total + shares[p - 1, at].astype(F32)
        if d == 0:
            back[mine] = total.astype(BF)
        else:
            summed[d] = total.astype(BF)
            c = remote(summed.at[d], back.at[mine], r_send.at[d], r_recv.at[d], "sp", at)
            c.start()
            back_copies.append(c)
    nxt = lax.rem(mine + 1, groups)
    prev_copy = remote(states_ref.at[pl.ds(toks - 8, 8)], prev_in, p_send, p_recv, "sp", nxt)
    prev_copy.start()
    advance(1, 0)
    while pieces:
        piece(*pieces.pop(0))
    rows = lax.broadcasted_iota(jnp.int32, (toks, toks), 0)
    cols = lax.broadcasted_iota(jnp.int32, (toks, toks), 1)
    eye = jnp.where(rows == cols, 1.0, 0.0).astype(BF)
    total = contract_rows(cot_ref[...], eye)
    for c in back_copies:
        c.wait_recv()
    total = total + contract_rows(back[...].reshape(size, width), picked)
    flipped[here, :] = total.astype(BF)
    grad_copies = []
    for d in range(1, parts):
        part = flipped.at[here]
        c = remote(part, part, g_send.at[d], g_recv.at[d], "tp", lax.rem(col + d, parts))
        c.start()
        grad_copies.append(c)
    for step in range(1, depth - 1):
        advance(1, step)
    collected(0)
    loads[5].wait()
    for c in grad_copies:
        c.wait_recv()
    high = model // groups
    block_copies = []
    for d in range(1, groups):
        peer = lax.rem(mine + d, groups)
        c = remote(flipped.at[near(high, peer)], blocks.at[mine], b_send.at[d], b_recv.at[d], "sp", peer)
        c.start()
        block_copies.append(c)
    grad_mixed = contract_rows(flipped[...], proj_all[...].reshape(model, states_ref.shape[1]))
    states = states_ref[...]
    act, branch_slope = gelu_parts(gate_ref[...].astype(F32))
    decays = jnp.exp(decay_ref[...])
    ggate_ref[...] = (grad_mixed * states * branch_slope).astype(BF)
    local = grad_mixed * act
    line = lax.broadcasted_iota(jnp.int32, local.shape, 0)
    span = jnp.where(line < toks - 1, pltpu.roll(decays, toks - 1, 0), 1.0)
    k = 1
    while k < toks:
        inside = line < toks - k
        local = local + span * jnp.where(inside, pltpu.roll(local, toks - k, 0), 0.0)
        span = span * jnp.where(inside, pltpu.roll(span, toks - k, 0), 1.0)
        k *= 2
    eight = lax.broadcasted_iota(jnp.int32, (8, local.shape[1]), 0)
    whole = span[0:1] * decays[0:1]
    entry = local[0:1] * decays[0:1]
    carry_own[...] = jnp.where(eight == 0, whole, entry)
    carry_copies = []
    for d in range(1, groups):
        peer = lax.rem(mine + d, groups)
        c = remote(carry_own, carry_in.at[d - 1], k_send.at[d], k_recv.at[d], "sp", peer)
        c.start()
        carry_copies.append(c)
    collected(1)
    total = jnp.dot(flipped[near(high, mine), :], mixed_all[mine], preferred_element_type=F32)
    for d in range(1, groups):
        block_copies[d - 1].wait_recv()
        at = lax.rem(mine + groups - d, groups)
        total = total + jnp.dot(blocks[at], mixed_all[at], preferred_element_type=F32)
    outp_ref[...] = total
    prev_copy.wait_recv()
    first = jnp.where(mine > 0, prev_in[7:8, :], 0.0)
    prev = jnp.where(line == 0, first, pltpu.roll(states, 1, 0))
    for c in carry_copies:
        c.wait_recv()
    carried = jnp.zeros_like(whole)
    for ahead in range(groups - 1, 0, -1):
        got = carry_in[groups - ahead - 1]
        carried = jnp.where(mine + ahead < groups, got[1:2] + got[0:1] * carried, carried)
    grad_in = local + span * carried
    gin_ref[...] = grad_in
    gdecay_ref[...] = (grad_in * decays * prev).astype(BF)
    settle(0)
    settle(1)
    for c in [prev_copy] + sends + back_copies + grad_copies + block_copies + carry_copies:
        c.wait_send()
    for o in stores:
        o.wait()


def shards(
    moe_input, cotangent, routes, route_weights, gate_branch, log_decay, states,
    w_gate, w_up, w_down, out_proj,
):
    groups, parts = lax.axis_size("sp"), lax.axis_size("tp")
    tok_rows, picks = routes.shape
    width = moe_input.shape[1]
    model = width * parts
    units = w_gate.shape[2]
    chans = states.shape[1]
    room = tok_rows * picks * 5 // (4 * groups)
    room = (room + 7) // 8 * 8
    depth = groups // CORES
    high = out_proj.shape[0]
    chunked = groups * parts <= 64
    chunks = groups if chunked else 1
    vmem = pl.BlockSpec(memory_space=pltpu.VMEM)
    hbm = pl.BlockSpec(memory_space=pl.ANY)
    dma = pltpu.SemaphoreType.DMA

    def run(*refs):
        whole_kernel(groups, parts, room, chunked, *refs)

    def buf(*shape, kind=BF):
        return pltpu.VMEM(shape, kind)

    outs = pl.pallas_call(
        run,
        out_shape=[
            jax.ShapeDtypeStruct((model, units), BF),
            jax.ShapeDtypeStruct((model, units), BF),
            jax.ShapeDtypeStruct((units, model), BF),
            jax.ShapeDtypeStruct((high, chans), F32),
            jax.ShapeDtypeStruct((tok_rows, chans), BF),
            jax.ShapeDtypeStruct((tok_rows, chans), BF),
            jax.ShapeDtypeStruct((tok_rows, chans), F32),
        ],
        in_specs=[vmem] * 2 + [hbm] * 9,
        out_specs=[hbm] * 3 + [vmem] * 4,
        scratch_shapes=[
            buf(tok_rows, width), buf(tok_rows, width), buf(tok_rows, chans),
            buf(tok_rows, chans, kind=F32), buf(tok_rows, chans, kind=F32),
            buf(model, units), buf(model, units), buf(units, model),
            buf(groups, room, width), buf(groups, room, width),
            buf(groups, room, model), buf(groups, room, model),
            buf(groups, high, chans), buf(groups, tok_rows, chans), buf(tok_rows, chans),
            buf(model, units), buf(model, units), buf(units, model),
            buf(parts, groups, room, width), buf(parts - 1, groups, room, width),
            buf(groups, room, width), buf(groups, room, width),
            buf(model, tok_rows), buf(groups, high, tok_rows),
            buf(8, chans, kind=F32), buf(groups - 1, 8, chans, kind=F32), buf(8, chans, kind=F32),
        ]
        + [dma((2, groups))] * 2 + [dma((2, chunks, parts))] * 2 + [dma((2, 2, depth))] * 4
        + [dma((chunks, parts))] * 2 + [dma((groups,))] * 2 + [dma((parts,))] * 2
        + [dma((groups,))] * 4 + [dma(())] * 2 + [dma((9,)), dma((4 + 3 * parts,))],
        compiler_params=pltpu.CompilerParams(
            collective_id=0, has_side_effects=True, vmem_limit_bytes=60 * 1024 * 1024),
        name="backward",
    )(
        routes.T, route_weights.T, moe_input, cotangent, gate_branch, states, log_decay, out_proj,
        w_gate, w_up, w_down,
    )
    return tuple(out.astype(F32)[None] for out in outs[:3]) + tuple(outs[3:])


def solution(mesh):
    return jax.shard_map(
        shards,
        mesh=mesh,
        in_specs=(
            P("sp", "tp"), P("sp", "tp"), P("sp", None), P("sp", None), P("sp", "tp"),
            P("sp", "tp"), P("sp", "tp"), P("sp", None, "tp"), P("sp", None, "tp"),
            P("sp", "tp", None), P("sp", "tp"),
        ),
        out_specs=(
            P("sp", None, "tp"), P("sp", None, "tp"), P("sp", "tp", None), P("sp", "tp"),
            P("sp", "tp"), P("sp", "tp"), P("sp", "tp"),
        ),
        check_vma=False,
    )
```

profile of v0, /device:TPU:0, one launch (start us, length us, event | category | flops | bytes accessed | tf_op | source)
XLA Modules:
  0.0 100.8 jit_solution(6210976582658520026)
XLA Ops:
  0.6 87.7 %backward.1 = (bf16[2048,512]{1,0:T(8,128)(2,1)}, bf16[2048,512]{1,0:T(8,128)(2,1)}, bf16[512,2048]{1,0:T(8,128)(2,1)}, f32[256,640]{1,0:T(8,128)}, bf16[128,640...) custom-call(s32[2,128]{1,0:T(2,128)} %bitcast.11, f32[2,128]{1,0:T(2,128)} %bitcast.12, ...), custom_call_target="tpu_custom_call" | custom-call | tf_op jit(solution)/shard_map/backward/pallas_call | solution.py:425
  88.3 0.0 copy-start
  88.3 7.0 %bitcast_convert_fusion.1 = (f32[1,2048,512]{2,1,0:T(8,128)}, f32[1,2048,512]{2,1,0:T(8,128)}) fusion(bf16[2048,512]{1,0:T(8,128)(2,1)} %get-tuple-element.15, bf16[2048,512]{1,0:T(8,128)(2,1)} %get-tuple-element.14), kind=kLoop, calls=%fused_computation.1 | loop fusion | flops 2097152 | bytes 12582912 | tf_op jit(solution)/shard_map/broadcast_in_dim | solution.py:461
  95.3 0.0 copy-done
  95.3 0.0 copy-start.1
  95.3 0.0 copy-start.4
  95.3 0.0 copy-start.3
  95.3 2.5 %bitcast_convert_fusion = f32[1,512,2048]{2,1,0:T(8,128)} fusion(bf16[512,2048]{1,0:T(8,128)(2,1)S(1)} %copy-done), kind=kLoop, calls=%fused_computation | loop fusion | flops 1048576 | bytes 6291456 | tf_op jit(solution)/shard_map/broadcast_in_dim | solution.py:461
  97.9 0.0 copy-start.2
  97.9 0.0 copy-done.1
  97.9 0.8 copy.22
  98.7 0.0 copy-done.4
  98.7 0.7 copy.23
  99.4 0.0 copy-done.3
  99.4 0.7 copy.24
  100.0 0.0 copy-done.2
  100.0 0.7 copy.25
Async XLA Ops:
  88.3 7.0 %copy-start = (bf16[512,2048]{1,0:T(8,128)(2,1)S(1)}, bf16[512,2048]{1,0:T(8,128)(2,1)}, u32[]{:S(2)}) copy-start(bf16[512,2048]{1,0:T(8,128)(2,1)} %get-tuple-element.16) | copy-start | bytes 6291460
  95.3 2.6 %copy-start.1 = (f32[256,640]{1,0:T(8,128)S(1)}, f32[256,640]{1,0:T(8,128)}, u32[]{:S(2)}) copy-start(f32[256,640]{1,0:T(8,128)} %get-tuple-element.33) | copy-start | bytes 1966084
  95.3 3.4 %copy-start.4 = (bf16[128,640]{1,0:T(8,128)(2,1)S(1)}, bf16[128,640]{1,0:T(8,128)(2,1)}, u32[]{:S(2)}) copy-start(bf16[128,640]{1,0:T(8,128)(2,1)} %get-tuple-element.34) | copy-start | bytes 491524
  95.3 4.1 %copy-start.3 = (bf16[128,640]{1,0:T(8,128)(2,1)S(1)}, bf16[128,640]{1,0:T(8,128)(2,1)}, u32[]{:S(2)}) copy-start(bf16[128,640]{1,0:T(8,128)(2,1)} %get-tuple-element.35) | copy-start | bytes 491524
  97.9 2.2 %copy-start.2 = (f32[128,640]{1,0:T(8,128)S(1)}, f32[128,640]{1,0:T(8,128)}, u32[]{:S(2)}) copy-start(f32[128,640]{1,0:T(8,128)} %get-tuple-element.36) | copy-start | bytes 983044
where the time goes:
time: 101 us
  Pallas kernels  87.7 us (87%)
  other arithmetic  9.51 us (9%)
  local copies, waits for them, and re-layouts  2.91 us (3%)
    pallas_call x1, Pallas kernels, shards(): pl.pallas_call(run, out_shape=[jax.ShapeDtypeStruct((model, units), BF),...  87.7 us
    broadcast_in_dim x2, other arithmetic, shards(): return tuple((out.astype(F32)[None] for out in outs[:3])) + tuple(outs[3:])  9.51 us
    unnamed x14, local copies, waits for them, and re-layouts  2.91 us

commit v1 on v0

--- a/solution.py
+++ b/solution.py
@@ -85,9 +85,9 @@
     groups, parts, room, chunked,
     routes_ref, weights_ref, x_any, cot_any, gate_any, states_any, decay_any, proj_any,
     wg_any, wu_any, wd_any,
-    gg_ref, gu_ref, gd_ref, outp_ref, ggate_ref, gdecay_ref, gin_ref,
+    rx_ref, rc_ref, hid_ref, gpg_ref, gpu_ref, outp_ref, ggate_ref, gdecay_ref, gin_ref,
     x_ref, cot_ref, gate_ref, states_ref, decay_ref, wg, wu, wd,
-    out_x, out_c, rows_x, rows_c, proj_all, mixed_all, mix_own, gg, gu, gd,
+    out_x, out_c, rows_x, rows_c, proj_all, mixed_all, mix_own, acts,
     terms, shares, summed, back, flipped, blocks, carry_own, carry_in, prev_in,
     a_send, a_recv, t_send, t_recv, z_send, z_recv, c_send, c_recv,
     s_send, s_recv, r_send, r_recv, g_send, g_recv, b_send, b_recv, k_send, k_recv, p_send, p_recv,
@@ -243,11 +243,21 @@
         loads[i].wait()
     for c in gathers[0]:
         c.wait_recv()
+    stores = []
+
+    def put(src, dst):
+        o = pltpu.make_async_copy(src, dst, w_sem.at[4 + len(stores)])
+        o.start()
+        stores.append(o)
+
+    put(rows_x, rx_ref)
     row_data = rows_x[...].reshape(size, model)
     pre_gate = jnp.dot(row_data, wg[...], preferred_element_type=F32)
     pre_up = jnp.dot(row_data, wu[...], preferred_element_type=F32)
     active, slope = silu_parts(pre_gate)
     hidden = (active * pre_up).astype(BF)
+    acts[0] = hidden
+    put(acts.at[0], hid_ref)
     lean = pre_up * slope
     advance(0, 0)
     if depth > 2:
@@ -257,6 +267,11 @@
     grad_hidden = contract_cols(rows_c[...].reshape(size, model), wd[...])
     grad_pre_gate = (grad_hidden * lean).astype(BF)
     grad_pre_up = (grad_hidden * active).astype(BF)
+    acts[1] = grad_pre_gate
+    acts[2] = grad_pre_up
+    put(rows_c, rc_ref)
+    put(acts.at[1], gpg_ref)
+    put(acts.at[2], gpu_ref)
     for d in list(range(1, parts)) + [0]:
         part = near(width, lax.rem(col + d, parts))
         term = contract_cols(grad_pre_gate, wg[part, :]) + contract_cols(grad_pre_up, wu[part, :])
@@ -278,26 +293,8 @@
     chain(1, 0)
     across(1, 0, 0, "start")
 
-    stores = []
-
-    def piece(kind, p):
-        part = slice(p * width, (p + 1) * width)
-        if kind == 2:
-            gd[:, part] = contract_rows(hidden, rows_c[:, :, part].reshape(size, width)).astype(BF)
-            s, t = gd.at[:, part], gd_ref.at[:, part]
-        else:
-            grad, buf, out = ((grad_pre_gate, gg, gg_ref), (grad_pre_up, gu, gu_ref))[kind]
-            buf[part, :] = contract_rows(rows_x[:, :, part].reshape(size, width), grad).astype(BF)
-            s, t = buf.at[part], out.at[part]
-        o = pltpu.make_async_copy(s, t, w_sem.at[4 + kind * parts + p])
-        o.start()
-        stores.append(o)
-
-    pieces = [(kind, p) for kind in range(3) for p in range(parts)]
     back_copies = []
     for d in order:
-        if pieces:
-            piece(*pieces.pop(0))
         at = lax.rem(mine + d, groups)
         if chunked or d == 1:
             for p in range(1, parts):
@@ -316,8 +313,6 @@
     prev_copy = remote(states_ref.at[pl.ds(toks - 8, 8)], prev_in, p_send, p_recv, "sp", nxt)
     prev_copy.start()
     advance(1, 0)
-    while pieces:
-        piece(*pieces.pop(0))
     rows = lax.broadcasted_iota(jnp.int32, (toks, toks), 0)
     cols = lax.broadcasted_iota(jnp.int32, (toks, toks), 1)
     eye = jnp.where(rows == cols, 1.0, 0.0).astype(BF)
@@ -396,6 +391,48 @@
         o.wait()
 
 
+def finish_kernel(
+    rx, rc, hid, gpg, gpu, outp, ggate, gdecay, gin,
+    gg_out, gu_out, gd_out, outp_out, ggate_out, gdecay_out, gin_out,
+):
+    gg_out[...] = contract_rows(rx[...], gpg[...])
+    gu_out[...] = contract_rows(rx[...], gpu[...])
+    gd_out[...] = contract_rows(hid[...], rc[...])
+    outp_out[...] = outp[...]
+    ggate_out[...] = ggate[...]
+    gdecay_out[...] = gdecay[...]
+    gin_out[...] = gin[...]
+
+
+def finish(rx, rc, hid, gpg, gpu, *small):
+    size, model = rx.shape
+    units = hid.shape[1]
+    steps = model // 256
+
+    def cols(rows):
+        return pl.BlockSpec((rows, 256), lambda i: (0, i))
+
+    def band(array):
+        return pl.BlockSpec((array.shape[0] // steps, array.shape[1]), lambda i: (i, 0))
+
+    full = pl.BlockSpec((size, units), lambda i: (0, 0))
+    tall = pl.BlockSpec((256, units), lambda i: (i, 0))
+    outs = pl.pallas_call(
+        finish_kernel,
+        grid=(steps,),
+        out_shape=[
+            jax.ShapeDtypeStruct((model, units), F32),
+            jax.ShapeDtypeStruct((model, units), F32),
+            jax.ShapeDtypeStruct((units, model), F32),
+        ] + [jax.ShapeDtypeStruct(a.shape, a.dtype) for a in small],
+        in_specs=[cols(size)] * 2 + [full] * 3 + [band(a) for a in small],
+        out_specs=[tall] * 2 + [cols(units)] + [band(a) for a in small],
+        compiler_params=pltpu.CompilerParams(vmem_limit_bytes=40 * 1024 * 1024),
+        name="finish",
+    )(rx, rc, hid, gpg, gpu, *small)
+    return tuple(out[None] for out in outs[:3]) + tuple(outs[3:])
+
+
 def shards(
     moe_input, cotangent, routes, route_weights, gate_branch, log_decay, states,
     w_gate, w_up, w_down, out_proj,
@@ -425,16 +462,18 @@
     outs = pl.pallas_call(
         run,
         out_shape=[
-            jax.ShapeDtypeStruct((model, units), BF),
-            jax.ShapeDtypeStruct((model, units), BF),
-            jax.ShapeDtypeStruct((units, model), BF),
+            jax.ShapeDtypeStruct((groups, room, model), BF),
+            jax.ShapeDtypeStruct((groups, room, model), BF),
+            jax.ShapeDtypeStruct((groups * room, units), BF),
+            jax.ShapeDtypeStruct((groups * room, units), BF),
+            jax.ShapeDtypeStruct((groups * room, units), BF),
             jax.ShapeDtypeStruct((high, chans), F32),
             jax.ShapeDtypeStruct((tok_rows, chans), BF),
             jax.ShapeDtypeStruct((tok_rows, chans), BF),
             jax.ShapeDtypeStruct((tok_rows, chans), F32),
         ],
         in_specs=[vmem] * 2 + [hbm] * 9,
-        out_specs=[hbm] * 3 + [vmem] * 4,
+        out_specs=[hbm] * 5 + [vmem] * 4,
         scratch_shapes=[
             buf(tok_rows, width), buf(tok_rows, width), buf(tok_rows, chans),
             buf(tok_rows, chans, kind=F32), buf(tok_rows, chans, kind=F32),
@@ -442,7 +481,7 @@
             buf(groups, room, width), buf(groups, room, width),
             buf(groups, room, model), buf(groups, room, model),
             buf(groups, high, chans), buf(groups, tok_rows, chans), buf(tok_rows, chans),
-            buf(model, units), buf(model, units), buf(units, model),
+            buf(3, groups * room, units),
             buf(parts, groups, room, width), buf(parts - 1, groups, room, width),
             buf(groups, room, width), buf(groups, room, width),
             buf(model, tok_rows), buf(groups, high, tok_rows),
@@ -450,7 +489,7 @@
         ]
         + [dma((2, groups))] * 2 + [dma((2, chunks, parts))] * 2 + [dma((2, 2, depth))] * 4
         + [dma((chunks, parts))] * 2 + [dma((groups,))] * 2 + [dma((parts,))] * 2
-        + [dma((groups,))] * 4 + [dma(())] * 2 + [dma((9,)), dma((4 + 3 * parts,))],
+        + [dma((groups,))] * 4 + [dma(())] * 2 + [dma((9,)), dma((9,))],
         compiler_params=pltpu.CompilerParams(
             collective_id=0, has_side_effects=True, vmem_limit_bytes=60 * 1024 * 1024),
         name="backward",
@@ -458,7 +497,8 @@
         routes.T, route_weights.T, moe_input, cotangent, gate_branch, states, log_decay, out_proj,
         w_gate, w_up, w_down,
     )
-    return tuple(out.astype(F32)[None] for out in outs[:3]) + tuple(outs[3:])
+    rx, rc = (out.reshape(groups * room, model) for out in outs[:2])
+    return finish(rx, rc, *outs[2:])
 
 
 def solution(mesh):

time: 101 us -> 106 us (1.050)
  other arithmetic: 9.51 us -> 0 us
  Pallas kernels: 87.7 us -> 95.2 us
  local copies, waits for them, and re-layouts: 2.91 us -> 9.43 us
    broadcast_in_dim x2 -> x0, other arithmetic: 9.51 us -> none  [shards(): return tuple((out.astype(F32)[None] for out in outs[:3])) + tuple(outs[3:])]
    pallas_call x1 -> x2, Pallas kernels: 87.7 us -> 95.2 us  [the longest x1 87.7 us: shards(): pl.pallas_call(run, out_shape=[jax.ShapeDtypeStruct((groups, room, model)...]
    unnamed x14 -> x18, local copies, waits for them, and re-layouts: 2.91 us -> 9.43 us
where the time goes in v1:
time: 106 us; the launch traced here: 105 us
  Pallas kernels  95.2 us (90%)
  local copies, waits for them, and re-layouts  9.43 us (9%)
    pallas_call x1, Pallas kernels, shards(): pl.pallas_call(run, out_shape=[jax.ShapeDtypeStruct((groups, room, model)...  87.7 us
    unnamed x18, local copies, waits for them, and re-layouts  9.43 us
    pallas_call x1, Pallas kernels, finish(): pl.pallas_call(finish_kernel, grid=(steps,), out_shape=[jax.ShapeDtypeStr...  7.46 us

profile of v1, /device:TPU:0, one launch (start us, length us, event | category | flops | bytes accessed | tf_op | source)
XLA Modules:
  0.0 105.3 jit_solution(14866216583213102550)
XLA Ops:
  0.6 87.7 %backward.1 = (bf16[8,40,2048]{2,1,0:T(8,128)(2,1)}, bf16[8,40,2048]{2,1,0:T(8,128)(2,1)}, bf16[320,512]{1,0:T(8,128)(2,1)}, bf16[320,512]{1,0:T(8,128)(2,1)}, b...) custom-call(s32[2,128]{1,0:T(2,128)} %bitcast.9, ...), custom_call_target="tpu_custom_call" | custom-call | tf_op jit(solution)/shard_map/backward/pallas_call | solution.py:462
  88.4 0.0 copy-start
  88.4 1.3 %copy-done = bf16[8,40,2048]{2,1,0:T(8,128)(2,1)S(1)} copy-done((bf16[8,40,2048]{2,1,0:T(8,128)(2,1)S(1)}, bf16[8,40,2048]{2,1,0:T(8,128)(2,1)}, u32[]{:S(2)}) %copy-start) | copy-done | bytes 1310744
  89.7 0.0 copy-start.1
  89.7 1.3 %copy-done.1 = bf16[8,40,2048]{2,1,0:T(8,128)(2,1)S(1)} copy-done((bf16[8,40,2048]{2,1,0:T(8,128)(2,1)S(1)}, bf16[8,40,2048]{2,1,0:T(8,128)(2,1)}, u32[]{:S(2)}) %copy-start.1) | copy-done | bytes 1310744
  91.0 0.0 copy-start.2
  91.0 1.1 %copy-done.2 = f32[256,640]{1,0:T(8,128)S(1)} copy-done((f32[256,640]{1,0:T(8,128)S(1)}, f32[256,640]{1,0:T(8,128)}, u32[]{:S(2)}) %copy-start.2) | copy-done | bytes 655384
  92.1 0.0 copy-start.3
  92.1 1.0 copy-done.3
  93.1 0.0 copy-start.4
  93.1 1.0 copy-done.4
  94.1 0.0 copy-start.5
  94.1 1.0 copy-done.5
  95.0 0.0 copy-start.6
  95.0 1.0 copy-done.6
  96.0 0.0 copy-start.7
  96.0 0.9 copy-done.7
  96.9 0.0 copy-start.8
  96.9 0.9 copy-done.8
  97.8 7.5 %finish.1 = (f32[2048,512]{1,0:T(8,128)}, f32[2048,512]{1,0:T(8,128)}, f32[512,2048]{1,0:T(8,128)}, f32[256,640]{1,0:T(8,128)}, bf16[128,640]{1,0:T(8,128)(2,1)}...) custom-call(bf16[320,2048]{1,0:T(8,128)(2,1)S(1)} %bitcast.7, bf16[320,2048]{1,0:T(8,128)(2,1)S(1)} %bitcast.8, ...), custom_call_target="tpu_custom_call" | custom-call | tf_op jit(solution)/shard_map/finish/pallas_call | solution.py:420
Async XLA Ops:
  88.4 1.3 %copy-start = (bf16[8,40,2048]{2,1,0:T(8,128)(2,1)S(1)}, bf16[8,40,2048]{2,1,0:T(8,128)(2,1)}, u32[]{:S(2)}) copy-start(bf16[8,40,2048]{2,1,0:T(8,128)(2,1)} %get-tuple-element.23) | copy-start | bytes 3932164
  89.7 1.3 %copy-start.1 = (bf16[8,40,2048]{2,1,0:T(8,128)(2,1)S(1)}, bf16[8,40,2048]{2,1,0:T(8,128)(2,1)}, u32[]{:S(2)}) copy-start(bf16[8,40,2048]{2,1,0:T(8,128)(2,1)} %get-tuple-element.24) | copy-start | bytes 3932164
  91.0 1.1 %copy-start.2 = (f32[256,640]{1,0:T(8,128)S(1)}, f32[256,640]{1,0:T(8,128)}, u32[]{:S(2)}) copy-start(f32[256,640]{1,0:T(8,128)} %get-tuple-element.28.outp) | copy-start | bytes 1966084
  92.1 1.0 copy-start.3
  93.1 1.0 copy-start.4
  94.1 1.0 copy-start.5
  95.0 1.0 copy-start.6
  96.0 0.9 copy-start.7
  96.9 0.9 copy-start.8

commit v2 on v1

--- a/solution.py
+++ b/solution.py
@@ -85,9 +85,9 @@
     groups, parts, room, chunked,
     routes_ref, weights_ref, x_any, cot_any, gate_any, states_any, decay_any, proj_any,
     wg_any, wu_any, wd_any,
-    rx_ref, rc_ref, hid_ref, gpg_ref, gpu_ref, outp_ref, ggate_ref, gdecay_ref, gin_ref,
+    rows_x, rows_c, hid_ref, gpg_ref, gpu_ref, outp_ref, ggate_ref, gdecay_ref, gin_ref,
     x_ref, cot_ref, gate_ref, states_ref, decay_ref, wg, wu, wd,
-    out_x, out_c, rows_x, rows_c, proj_all, mixed_all, mix_own, acts,
+    out_x, out_c, proj_all, mixed_all, mix_own,
     terms, shares, summed, back, flipped, blocks, carry_own, carry_in, prev_in,
     a_send, a_recv, t_send, t_recv, z_send, z_recv, c_send, c_recv,
     s_send, s_recv, r_send, r_recv, g_send, g_recv, b_send, b_recv, k_send, k_recv, p_send, p_recv,
@@ -243,21 +243,12 @@
         loads[i].wait()
     for c in gathers[0]:
         c.wait_recv()
-    stores = []
-
-    def put(src, dst):
-        o = pltpu.make_async_copy(src, dst, w_sem.at[4 + len(stores)])
-        o.start()
-        stores.append(o)
-
-    put(rows_x, rx_ref)
     row_data = rows_x[...].reshape(size, model)
     pre_gate = jnp.dot(row_data, wg[...], preferred_element_type=F32)
     pre_up = jnp.dot(row_data, wu[...], preferred_element_type=F32)
     active, slope = silu_parts(pre_gate)
     hidden = (active * pre_up).astype(BF)
-    acts[0] = hidden
-    put(acts.at[0], hid_ref)
+    hid_ref[...] = hidden
     lean = pre_up * slope
     advance(0, 0)
     if depth > 2:
@@ -267,11 +258,8 @@
     grad_hidden = contract_cols(rows_c[...].reshape(size, model), wd[...])
     grad_pre_gate = (grad_hidden * lean).astype(BF)
     grad_pre_up = (grad_hidden * active).astype(BF)
-    acts[1] = grad_pre_gate
-    acts[2] = grad_pre_up
-    put(rows_c, rc_ref)
-    put(acts.at[1], gpg_ref)
-    put(acts.at[2], gpu_ref)
+    gpg_ref[...] = grad_pre_gate
+    gpu_ref[...] = grad_pre_up
     for d in list(range(1, parts)) + [0]:
         part = near(width, lax.rem(col + d, parts))
         term = contract_cols(grad_pre_gate, wg[part, :]) + contract_cols(grad_pre_up, wu[part, :])
@@ -387,8 +375,6 @@
     settle(1)
     for c in [prev_copy] + sends + back_copies + grad_copies + block_copies + carry_copies:
         c.wait_send()
-    for o in stores:
-        o.wait()
 
 
 def finish_kernel(
@@ -450,7 +436,7 @@
     chunked = groups * parts <= 64
     chunks = groups if chunked else 1
     vmem = pl.BlockSpec(memory_space=pltpu.VMEM)
-    hbm = pl.BlockSpec(memory_space=pl.ANY)
+    hbm = pl.BlockSpec(memory_space=pltpu.HBM)
     dma = pltpu.SemaphoreType.DMA
 
     def run(*refs):
@@ -473,15 +459,13 @@
             jax.ShapeDtypeStruct((tok_rows, chans), F32),
         ],
         in_specs=[vmem] * 2 + [hbm] * 9,
-        out_specs=[hbm] * 5 + [vmem] * 4,
+        out_specs=[vmem] * 9,
         scratch_shapes=[
             buf(tok_rows, width), buf(tok_rows, width), buf(tok_rows, chans),
             buf(tok_rows, chans, kind=F32), buf(tok_rows, chans, kind=F32),
             buf(model, units), buf(model, units), buf(units, model),
             buf(groups, room, width), buf(groups, room, width),
-            buf(groups, room, model), buf(groups, room, model),
             buf(groups, high, chans), buf(groups, tok_rows, chans), buf(tok_rows, chans),
-            buf(3, groups * room, units),
             buf(parts, groups, room, width), buf(parts - 1, groups, room, width),
             buf(groups, room, width), buf(groups, room, width),
             buf(model, tok_rows), buf(groups, high, tok_rows),
@@ -489,13 +473,14 @@
         ]
         + [dma((2, groups))] * 2 + [dma((2, chunks, parts))] * 2 + [dma((2, 2, depth))] * 4
         + [dma((chunks, parts))] * 2 + [dma((groups,))] * 2 + [dma((parts,))] * 2
-        + [dma((groups,))] * 4 + [dma(())] * 2 + [dma((9,)), dma((9,))],
+        + [dma((groups,))] * 4 + [dma(())] * 2 + [dma((9,)), dma((4,))],
         compiler_params=pltpu.CompilerParams(
-            collective_id=0, has_side_effects=True, vmem_limit_bytes=60 * 1024 * 1024),
+            collective_id=0, has_side_effects=True, vmem_limit_bytes=40 * 1024 * 1024),
         name="backward",
     )(
-        routes.T, route_weights.T, moe_input, cotangent, gate_branch, states, log_decay, out_proj,
-        w_gate, w_up, w_down,
+        routes.T, route_weights.T,
+        *(pltpu.with_memory_space_constraint(a, pltpu.HBM) for a in (
+            moe_input, cotangent, gate_branch, states, log_decay, out_proj, w_gate, w_up, w_down)),
     )
     rx, rc = (out.reshape(groups * room, model) for out in outs[:2])
     return finish(rx, rc, *outs[2:])

time: 106 us -> 95.5 us (0.901)
  local copies, waits for them, and re-layouts: 9.43 us -> 1.35 us
  Pallas kernels: 95.2 us -> 93.4 us
    unnamed x18 -> x4, local copies, waits for them, and re-layouts: 9.43 us -> 1.35 us
    pallas_call x1, Pallas kernels: 87.7 us -> 85.9 us  [shards(): pl.pallas_call(run, out_shape=[jax.ShapeDtypeStruct((groups, room, model)...]
where the time goes in v2:
time: 95.5 us; the launch traced here: 95.4 us
  Pallas kernels  93.4 us (98%)
  local copies, waits for them, and re-layouts  1.35 us (1%)
    pallas_call x1, Pallas kernels, shards(): pl.pallas_call(run, out_shape=[jax.ShapeDtypeStruct((groups, room, model)...  85.9 us
    pallas_call x1, Pallas kernels, finish(): pl.pallas_call(finish_kernel, grid=(steps,), out_shape=[jax.ShapeDtypeStr...  7.48 us

profile of v2, /device:TPU:0, one launch (start us, length us, event | category | flops | bytes accessed | tf_op | source)
XLA Modules:
  0.0 95.4 jit_solution(7628082054972752164)
XLA Ops:
  0.6 0.0 copy-start
  0.6 0.7 copy-done
  1.3 0.0 copy-start.1
  1.3 0.7 copy-done.1
  2.0 85.9 %backward.1 = (bf16[8,40,2048]{2,1,0:T(8,128)(2,1)S(1)}, bf16[8,40,2048]{2,1,0:T(8,128)(2,1)S(1)}, bf16[320,512]{1,0:T(8,128)(2,1)S(1)}, bf16[320,512]{1,0:T(8,1...) custom-call(s32[2,128]{1,0:T(2,128)S(1)} %bitcast.9, ...), custom_call_target="tpu_custom_call" | custom-call | tf_op jit(solution)/shard_map/backward/pallas_call | solution.py:448
  87.9 7.5 %finish.1 = (f32[2048,512]{1,0:T(8,128)}, f32[2048,512]{1,0:T(8,128)}, f32[512,2048]{1,0:T(8,128)}, f32[256,640]{1,0:T(8,128)}, bf16[128,640]{1,0:T(8,128)(2,1)}...) custom-call(bf16[320,2048]{1,0:T(8,128)(2,1)S(1)} %bitcast.7, bf16[320,2048]{1,0:T(8,128)(2,1)S(1)} %bitcast.8, ...), custom_call_target="tpu_custom_call" | custom-call | tf_op jit(solution)/shard_map/finish/pallas_call | solution.py:406
Async XLA Ops:
  0.6 0.7 copy-start
  1.3 0.7 copy-start.1

commit v3 on v2

--- a/solution.py
+++ b/solution.py
@@ -380,39 +380,47 @@
 def finish_kernel(
     rx, rc, hid, gpg, gpu, outp, ggate, gdecay, gin,
     gg_out, gu_out, gd_out, outp_out, ggate_out, gdecay_out, gin_out,
+    gg, gu, gd, sems, small_sems,
 ):
-    gg_out[...] = contract_rows(rx[...], gpg[...])
-    gu_out[...] = contract_rows(rx[...], gpu[...])
-    gd_out[...] = contract_rows(hid[...], rc[...])
-    outp_out[...] = outp[...]
-    ggate_out[...] = ggate[...]
-    gdecay_out[...] = gdecay[...]
-    gin_out[...] = gin[...]
+    stores = []
+    for i, (src, dst) in enumerate((
+        (outp, outp_out), (ggate, ggate_out), (gdecay, gdecay_out), (gin, gin_out),
+    )):
+        o = pltpu.make_async_copy(src, dst, small_sems.at[i])
+        o.start()
+        stores.append(o)
+    steps = sems.shape[1]
+    step = rx.shape[1] // steps
+    for i in range(steps):
+        part = slice(i * step, (i + 1) * step)
+        for kind, grad, buf, out in ((0, gpg, gg, gg_out), (1, gpu, gu, gu_out)):
+            buf[part, :] = contract_rows(rx[:, part], grad[...])
+            o = pltpu.make_async_copy(buf.at[part], out.at[part], sems.at[kind, i])
+            o.start()
+            stores.append(o)
+        gd[:, part] = contract_rows(hid[...], rc[:, part])
+        o = pltpu.make_async_copy(gd.at[:, part], gd_out.at[:, part], sems.at[2, i])
+        o.start()
+        stores.append(o)
+    for o in stores:
+        o.wait()
 
 
 def finish(rx, rc, hid, gpg, gpu, *small):
     size, model = rx.shape
     units = hid.shape[1]
     steps = model // 256
-
-    def cols(rows):
-        return pl.BlockSpec((rows, 256), lambda i: (0, i))
-
-    def band(array):
-        return pl.BlockSpec((array.shape[0] // steps, array.shape[1]), lambda i: (i, 0))
-
-    full = pl.BlockSpec((size, units), lambda i: (0, 0))
-    tall = pl.BlockSpec((256, units), lambda i: (i, 0))
+    vmem = pl.BlockSpec(memory_space=pltpu.VMEM)
+    hbm = pl.BlockSpec(memory_space=pltpu.HBM)
+    grads = [(model, units), (model, units), (units, model)]
     outs = pl.pallas_call(
         finish_kernel,
-        grid=(steps,),
-        out_shape=[
-            jax.ShapeDtypeStruct((model, units), F32),
-            jax.ShapeDtypeStruct((model, units), F32),
-            jax.ShapeDtypeStruct((units, model), F32),
-        ] + [jax.ShapeDtypeStruct(a.shape, a.dtype) for a in small],
-        in_specs=[cols(size)] * 2 + [full] * 3 + [band(a) for a in small],
-        out_specs=[tall] * 2 + [cols(units)] + [band(a) for a in small],
+        out_shape=[jax.ShapeDtypeStruct(g, F32) for g in grads]
+        + [jax.ShapeDtypeStruct(a.shape, a.dtype) for a in small],
+        in_specs=[vmem] * (5 + len(small)),
+        out_specs=[hbm] * (3 + len(small)),
+        scratch_shapes=[pltpu.VMEM(g, F32) for g in grads]
+        + [pltpu.SemaphoreType.DMA((3, steps)), pltpu.SemaphoreType.DMA((len(small),))],
         compiler_params=pltpu.CompilerParams(vmem_limit_bytes=40 * 1024 * 1024),
         name="finish",
     )(rx, rc, hid, gpg, gpu, *small)
@@ -486,9 +494,477 @@
     return finish(rx, rc, *outs[2:])
 
 
+def flip(index, mask, count):
+    total, bit = 0, 1
+    while bit < count:
+        here = lax.rem(lax.div(index, bit), 2)
+        total = total + bit * ((1 - here) if mask & bit else here)
+        bit *= 2
+    return total
+
+
+def plane_kernel(
+    groups, parts, room,
+    routes_any, weights_any, x_any, cot_any, gate_any, states_any, decay_any, proj_any,
+    wg_any, wu_any, wd_any,
+    rows_x, rows_c, hid_ref, gpg_ref, gpu_ref, outp_ref, ggate_ref, gdecay_ref, gin_ref,
+    routes_ref, weights_ref, x_ref, cot_ref, gate_ref, states_ref, decay_ref, wg, wu, wd,
+    out_x, out_c, picked_ref, proj_all, mixed_all, act_ref, slope_ref, active_ref, lean_ref,
+    terms, shares, summed, back, cot_turned, cot_mine, flipped, blocks, levels, span_ref, past_ref,
+    carry_own, carry_in, prev_in,
+    a_send, a_recv, t_send, t_recv, z_send, z_recv, c_send, c_recv,
+    s_send, s_recv, r_send, r_recv, g_send, g_recv, b_send, b_recv, q_send, q_recv, u_send, u_recv,
+    k_send, k_recv, p_send, p_recv, l_sem,
+):
+    mine, col = lax.axis_index("sp"), lax.axis_index("tp")
+    toks, width = x_ref.shape
+    model = rows_x.shape[2]
+    chans = states_ref.shape[1]
+    units = hid_ref.shape[2]
+    depth = groups // CORES
+    z, core = mine // CORES, lax.rem(mine, CORES)
+    size = groups * room
+    half = groups // 2
+    rows_half = half * room
+    started = []
+
+    barrier = pltpu.get_barrier_semaphore()
+    for d in range(1, groups):
+        pl.semaphore_signal(
+            barrier, inc=1, device_id={"sp": lax.rem(mine + d, groups)},
+            device_id_type=pl.DeviceIdType.MESH,
+        )
+    for d in range(1, parts):
+        pl.semaphore_signal(
+            barrier, inc=1, device_id={"tp": lax.rem(col + d, parts)},
+            device_id_type=pl.DeviceIdType.MESH,
+        )
+
+    loads = []
+    for i, (s, t) in enumerate((
+        (x_any, x_ref), (cot_any, cot_ref), (gate_any, gate_ref), (states_any, states_ref),
+        (proj_any, proj_all.at[mine]), (decay_any, decay_ref),
+        (wg_any.at[0], wg), (wu_any.at[0], wu), (wd_any.at[0], wd),
+        (routes_any, routes_ref), (weights_any, weights_ref),
+    )):
+        loads.append(pltpu.make_async_copy(s, t, l_sem.at[i]))
+    for i in (9, 10, 0, 1, 4, 2, 3, 6, 7, 8, 5):
+        loads[i].start()
+
+    def near(width_of, index):
+        return pl.ds(pl.multiple_of(index * width_of, width_of), width_of)
+
+    def send(src, dst, send_sem, recv_sem, axis, peer):
+        c = remote(src, dst, send_sem, recv_sem, axis, peer)
+        c.start()
+        started.append(c)
+        return c
+
+    group = [flip(mine, d, groups) for d in range(groups)]
+    tile = [flip(col, p, parts) for p in range(parts)]
+    here = near(width, col)
+
+    loads[9].wait()
+    loads[10].wait()
+    picked, weight = selection(routes_ref[...], weights_ref[...], groups, room)
+    picked_ref[...] = picked
+    arrivals = [[None] * groups for _ in range(2)]
+    gathers = [[None] * groups for _ in range(2)]
+    sources = ((out_x, rows_x), (out_c, rows_c))
+
+    def spread(a):
+        src, dst = sources[a]
+        for d in range(1, groups):
+            arrivals[a][d] = send(
+                src.at[group[d]], dst.at[mine, :, here], a_send.at[a, d], a_recv.at[a, d], "sp", group[d])
+        dst[mine, :, here] = src[mine]
+
+    def share_out(a, d):
+        src, dst = sources[a]
+        if d:
+            arrivals[a][d].wait_recv()
+        own = dst.at[group[d], :, here] if d else src.at[mine]
+        gathers[a][d] = [
+            send(own, dst.at[group[d], :, here], t_send.at[a, d, k], t_recv.at[a, d, k], "tp", tile[k + 1])
+            for k in range(2)
+        ]
+
+    def relay(a, d):
+        dst = sources[a][1]
+        k = d % 2
+        gathers[a][d][k].wait_recv()
+        ref = dst.at[group[d], :, near(width, tile[k + 1])]
+        gathers[a][d].append(
+            send(ref, ref, t_send.at[a, d, 2], t_recv.at[a, d, 2], "tp", tile[2 - k]))
+
+    def landed(a, d):
+        gathers[a][d][1 - d % 2].wait_recv()
+        gathers[a][d][2].wait_recv()
+
+    loads[0].wait()
+    got = jnp.dot(picked, x_ref[...], preferred_element_type=F32).astype(BF)
+    for e in range(groups):
+        out_x[e] = got[e * room : (e + 1) * room]
+    pl.semaphore_wait(barrier, groups + parts - 2)
+    spread(0)
+    share_out(0, 0)
+    loads[1].wait()
+    got = jnp.dot(picked, cot_ref[...], preferred_element_type=F32)
+    got = (got * weight).astype(BF)
+    for e in range(groups):
+        out_c[e] = got[e * room : (e + 1) * room]
+    spread(1)
+
+    pairs = (proj_all, mixed_all)
+
+    def chain(a, step, wait=False):
+        buf = pairs[a]
+        right = buf.at[jnp.maximum(z - step, 0) * CORES + core]
+        left = buf.at[jnp.minimum(z + step, depth - 1) * CORES + core]
+        up = jnp.minimum(z + 1, depth - 1) * CORES + core
+        down = jnp.maximum(z - 1, 0) * CORES + core
+        for way, ref, peer, ok in (
+            (0, right, up, jnp.logical_and(z - step >= 0, z + 1 < depth)),
+            (1, left, down, jnp.logical_and(z + step < depth, z >= 1)),
+        ):
+            @pl.when(ok)
+            def _(way=way, ref=ref, peer=peer):
+                c = remote(ref, ref, z_send.at[a, way, step], z_recv.at[a, way, step], "sp", peer)
+                c.wait_send() if wait else c.start()
+
+    partner = z * CORES + (1 - core)
+
+    def across(a, step, way, mode):
+        ok = z - step >= 0 if way == 0 else z + step < depth
+        zz = jnp.maximum(z - step, 0) if way == 0 else jnp.minimum(z + step, depth - 1)
+        ref = pairs[a].at[zz * CORES + (1 - core if mode == "recv" else core)]
+
+        @pl.when(ok)
+        def _():
+            c = remote(ref, ref, c_send.at[a, way, step], c_recv.at[a, way, step], "sp", partner)
+            if mode == "start":
+                c.start()
+            elif mode == "send":
+                c.wait_send()
+            else:
+                c.wait_recv()
+
+    def advance(a, step):
+        buf = pairs[a]
+        from_l = buf.at[jnp.maximum(z - 1 - step, 0) * CORES + core]
+        from_r = buf.at[jnp.minimum(z + 1 + step, depth - 1) * CORES + core]
+        for way, ok, ref in ((0, z - 1 - step >= 0, from_l), (1, z + 1 + step < depth, from_r)):
+            @pl.when(ok)
+            def _(way=way, ref=ref):
+                remote(ref, ref, z_send.at[a, way, step], z_recv.at[a, way, step],
+                       "sp", lax.rem(mine + 1, groups)).wait_recv()
+        if step + 1 < depth - 1:
+            chain(a, step + 1)
+        across(a, step + 1, 0, "start")
+        across(a, step + 1, 1, "start")
+
+    def settle(a):
+        for step in range(depth - 1):
+            chain(a, step, True)
+        for step in range(depth):
+            for way in range(2):
+                if step or not way:
+                    across(a, step, way, "send")
+
+    def collected(a):
+        for step in range(depth):
+            for way in range(2):
+                if step or not way:
+                    across(a, step, way, "recv")
+
+    loads[4].wait()
+    chain(0, 0)
+    across(0, 0, 0, "start")
+    loads[3].wait()
+    prev_copy = send(
+        states_ref.at[pl.ds(toks - 8, 8)], prev_in, p_send, p_recv, "sp", lax.rem(mine + 1, groups))
+
+    share_out(0, 1)
+    loads[2].wait()
+    act, branch_slope = gelu_parts(gate_ref[...].astype(F32))
+    states = states_ref[...]
+    act_ref[...] = act
+    slope_ref[...] = branch_slope * states
+    mixed_all[mine] = (act * states).astype(BF)
+    for d in range(2, groups):
+        share_out(0, d)
+        relay(0, d - 2)
+    share_out(1, 0)
+    relay(0, groups - 2)
+    share_out(1, 1)
+    relay(0, groups - 1)
+
+    first = [lax.div(mine, half) * half, (1 - lax.div(mine, half)) * half]
+
+    def forward(h):
+        for d in range(h * half, (h + 1) * half):
+            landed(0, d)
+        at = pl.ds(first[h], half)
+        data = rows_x[at].reshape(rows_half, model)
+        pre_gate = jnp.dot(data, wg[...].reshape(model, units), preferred_element_type=F32)
+        pre_up = jnp.dot(data, wu[...].reshape(model, units), preferred_element_type=F32)
+        active, slope = silu_parts(pre_gate)
+        hid_ref[at] = (active * pre_up).astype(BF).reshape(half, room, units)
+        active_ref[h] = active
+        lean_ref[h] = pre_up * slope
+
+    def hidden_grads(h):
+        for d in range(h * half, (h + 1) * half):
+            landed(1, d)
+        at = pl.ds(first[h], half)
+        grad_hidden = contract_cols(rows_c[at].reshape(rows_half, model), wd[...])
+        gpg_ref[at] = (grad_hidden * lean_ref[h]).astype(BF).reshape(half, room, units)
+        gpu_ref[at] = (grad_hidden * active_ref[h]).astype(BF).reshape(half, room, units)
+
+    def input_grads(h):
+        at = pl.ds(first[h], half)
+        gate_part = gpg_ref[at].reshape(rows_half, units)
+        up_part = gpu_ref[at].reshape(rows_half, units)
+        for p in list(range(1, parts)) + [0]:
+            term = contract_cols(gate_part, wg[:, tile[p]].reshape(width, units))
+            term = term + contract_cols(up_part, wu[:, tile[p]].reshape(width, units))
+            terms[p, at] = term.astype(BF).reshape(half, room, width)
+
+    share_copies = {}
+
+    def reduce_out(d):
+        for p in range(1, parts):
+            share_copies[d, p] = send(
+                terms.at[p, group[d]], shares.at[p - 1, group[d]],
+                s_send.at[d, p], s_recv.at[d, p], "tp", tile[p])
+
+    late = list(range(2, groups))
+    waiting = list(range(groups))
+
+    def pump(count):
+        for _ in range(count):
+            if late:
+                share_out(1, late.pop(0))
+            if waiting and (not late or waiting[0] <= late[0] - 3):
+                relay(1, waiting.pop(0))
+
+    pump(2)
+    for i in (6, 7, 8):
+        loads[i].wait()
+    forward(0)
+    pump(2)
+    forward(1)
+    pump(2)
+
+    rows = lax.broadcasted_iota(jnp.int32, (toks, toks), 0)
+    cols = lax.broadcasted_iota(jnp.int32, (toks, toks), 1)
+    eye = jnp.where(rows == cols, 1.0, 0.0).astype(BF)
+    fine = cot_turned.shape[2]
+    cot_turned[...] = contract_rows(cot_ref[...], eye).astype(BF).reshape(cot_turned.shape)
+    cot_mine[col] = cot_turned[:, col]
+
+    while len(waiting) > 2:
+        relay(1, waiting.pop(0))
+    hidden_grads(0)
+    while waiting:
+        relay(1, waiting.pop(0))
+    cot_copies = [
+        send(cot_turned.at[:, tile[p]], cot_mine.at[col], u_send.at[p], u_recv.at[p], "tp", tile[p])
+        for p in range(1, parts)
+    ]
+    input_grads(0)
+    for d in range(1, half):
+        reduce_out(d)
+    hidden_grads(1)
+    input_grads(1)
+    for d in list(range(half, groups)) + [0]:
+        reduce_out(d)
+    advance(0, 0)
+
+    loads[5].wait()
+    prev_copy.wait_recv()
+    decays = jnp.exp(decay_ref[...])
+    line = lax.broadcasted_iota(jnp.int32, decays.shape, 0)
+    before = jnp.where(mine > 0, prev_in[7:8, :], 0.0)
+    past_ref[...] = decays * jnp.where(line == 0, before, pltpu.roll(states_ref[...], 1, 0))
+    span = jnp.where(line < toks - 1, pltpu.roll(decays, toks - 1, 0), 1.0)
+    k, level = 1, 0
+    while k < toks:
+        inside = line < toks - k
+        levels[level] = jnp.where(inside, span, 0.0)
+        span = span * jnp.where(inside, pltpu.roll(span, toks - k, 0), 1.0)
+        k *= 2
+        level += 1
+    span_ref[...] = span
+    head = decays[0:1]
+
+    for i, d in enumerate(list(range(1, groups)) + [0]):
+        for p in range(1, parts):
+            share_copies[d, p].wait_recv()
+        total = terms[0, group[d]].astype(F32)
+        for p in range(1, parts):
+            total = total + shares[p - 1, group[d]].astype(F32)
+        if d == 0:
+            back[mine] = total.astype(BF)
+        else:
+            summed[d] = total.astype(BF)
+            arrivals[0][d] = send(
+                summed.at[d], back.at[mine], r_send.at[d], r_recv.at[d], "sp", group[d])
+        if i == half:
+            for step in range(1, depth - 1):
+                advance(0, step)
+            chain(1, 0)
+            across(1, 0, 0, "start")
+    advance(1, 0)
+    for c in cot_copies:
+        c.wait_recv()
+    total = cot_mine[...].reshape(width, toks).astype(F32)
+    for d in range(1, groups):
+        arrivals[0][d].wait_recv()
+    total = total + contract_rows(back[...].reshape(size, width), picked_ref[...])
+    flipped[:, col] = total.astype(BF).reshape(groups, fine, toks)
+    grad_copies = []
+    for p in range(1, parts):
+        part = flipped.at[:, col]
+        grad_copies.append(send(part, part, g_send.at[p], g_recv.at[p], "tp", tile[p]))
+    block_copies = [
+        send(flipped.at[group[d], col], blocks.at[mine, col], b_send.at[d], b_recv.at[d], "sp", group[d])
+        for d in range(1, groups)
+    ]
+    blocks[mine, col] = flipped[mine, col]
+    for step in range(1, depth - 1):
+        advance(1, step)
+    for c in block_copies:
+        c.wait_recv()
+    plane_copies = []
+    for p in range(1, parts):
+        part = blocks.at[:, col]
+        plane_copies.append(send(part, part, q_send.at[p], q_recv.at[p], "tp", tile[p]))
+    collected(0)
+    for c in grad_copies:
+        c.wait_recv()
+    grad_mixed = contract_rows(flipped[...].reshape(model, toks), proj_all[...].reshape(model, chans))
+    ggate_ref[...] = (grad_mixed * slope_ref[...]).astype(BF)
+    local = grad_mixed * act_ref[...]
+    k, level = 1, 0
+    while k < toks:
+        local = local + levels[level] * pltpu.roll(local, toks - k, 0)
+        k *= 2
+        level += 1
+    eight = lax.broadcasted_iota(jnp.int32, (8, chans), 0)
+    carry_own[...] = jnp.where(eight == 0, span_ref[0:1, :] * head, local[0:1] * head)
+    carry_copies = []
+    for d in range(1, groups):
+        peer = lax.rem(mine + d, groups)
+        carry_copies.append(
+            send(carry_own, carry_in.at[d - 1], k_send.at[d], k_recv.at[d], "sp", peer))
+    collected(1)
+    for c in plane_copies:
+        c.wait_recv()
+    high = blocks.shape[1] * blocks.shape[2]
+    total = jnp.zeros((high, chans), F32)
+    for t in range(groups):
+        total = total + jnp.dot(
+            blocks[t].reshape(high, toks), mixed_all[t], preferred_element_type=F32)
+    outp_ref[...] = total
+    for c in carry_copies:
+        c.wait_recv()
+    carried = jnp.zeros((1, chans), F32)
+    for ahead in range(groups - 1, 0, -1):
+        got = carry_in[groups - ahead - 1]
+        carried = jnp.where(mine + ahead < groups, got[1:2] + got[0:1] * carried, carried)
+    grad_in = local + span_ref[...] * carried
+    gin_ref[...] = grad_in
+    gdecay_ref[...] = (grad_in * past_ref[...]).astype(BF)
+    settle(0)
+    settle(1)
+    for c in started:
+        c.wait_send()
+
+
+def plane_shards(
+    moe_input, cotangent, routes, route_weights, gate_branch, log_decay, states,
+    w_gate, w_up, w_down, out_proj,
+):
+    groups, parts = lax.axis_size("sp"), lax.axis_size("tp")
+    tok_rows, picks = routes.shape
+    width = moe_input.shape[1]
+    model = width * parts
+    units = w_gate.shape[2]
+    chans = states.shape[1]
+    room = tok_rows * picks * 5 // (4 * groups)
+    room = (room + 7) // 8 * 8
+    depth = groups // CORES
+    high = out_proj.shape[0]
+    fine = high // parts
+    doublings = (tok_rows - 1).bit_length()
+    vmem = pl.BlockSpec(memory_space=pltpu.VMEM)
+    hbm = pl.BlockSpec(memory_space=pltpu.HBM)
+    dma = pltpu.SemaphoreType.DMA
+
+    def run(*refs):
+        plane_kernel(groups, parts, room, *refs)
+
+    def buf(*shape, kind=BF):
+        return pltpu.VMEM(shape, kind)
+
+    def split(weight):
+        return weight.reshape(1, groups, parts, fine, units)
+
+    outs = pl.pallas_call(
+        run,
+        out_shape=[
+            jax.ShapeDtypeStruct((groups, room, model), BF),
+            jax.ShapeDtypeStruct((groups, room, model), BF),
+            jax.ShapeDtypeStruct((groups, room, units), BF),
+            jax.ShapeDtypeStruct((groups, room, units), BF),
+            jax.ShapeDtypeStruct((groups, room, units), BF),
+            jax.ShapeDtypeStruct((high, chans), F32),
+            jax.ShapeDtypeStruct((tok_rows, chans), BF),
+            jax.ShapeDtypeStruct((tok_rows, chans), BF),
+            jax.ShapeDtypeStruct((tok_rows, chans), F32),
+        ],
+        in_specs=[hbm] * 11,
+        out_specs=[vmem] * 9,
+        scratch_shapes=[
+            buf(picks, tok_rows, kind=jnp.int32), buf(picks, tok_rows, kind=F32),
+            buf(tok_rows, width), buf(tok_rows, width), buf(tok_rows, chans),
+            buf(tok_rows, chans, kind=F32), buf(tok_rows, chans, kind=F32),
+            buf(groups, parts, fine, units), buf(groups, parts, fine, units), buf(units, model),
+            buf(groups, room, width), buf(groups, room, width), buf(groups * room, tok_rows),
+            buf(groups, high, chans), buf(groups, tok_rows, chans),
+            buf(tok_rows, chans, kind=F32), buf(tok_rows, chans, kind=F32),
+            buf(2, groups // 2 * room, units, kind=F32), buf(2, groups // 2 * room, units, kind=F32),
+            buf(parts, groups, room, width), buf(parts - 1, groups, room, width),
+            buf(groups, room, width), buf(groups, room, width),
+            buf(groups // parts, parts, fine, tok_rows), buf(parts, groups // parts, fine, tok_rows),
+            buf(groups, parts, fine, tok_rows), buf(groups, parts, fine, tok_rows),
+            buf(doublings, tok_rows, chans, kind=F32), buf(tok_rows, chans, kind=F32),
+            buf(tok_rows, chans, kind=F32),
+            buf(8, chans, kind=F32), buf(groups - 1, 8, chans, kind=F32), buf(8, chans, kind=F32),
+        ]
+        + [dma((2, groups))] * 2 + [dma((2, groups, 3))] * 2 + [dma((2, 2, depth))] * 4
+        + [dma((groups, parts))] * 2 + [dma((groups,))] * 2 + [dma((parts,))] * 2
+        + [dma((groups,))] * 2 + [dma((parts,))] * 4
+        + [dma((groups,))] * 2 + [dma(())] * 2 + [dma((11,))],
+        compiler_params=pltpu.CompilerParams(
+            collective_id=0, has_side_effects=True, vmem_limit_bytes=40 * 1024 * 1024),
+        name="backward",
+    )(
+        *(pltpu.with_memory_space_constraint(a, pltpu.HBM) for a in (
+            routes.T, route_weights.T, moe_input, cotangent, gate_branch, states, log_decay, out_proj,
+            split(w_gate), split(w_up), w_down)),
+    )
+    rx, rc = (out.reshape(groups * room, model) for out in outs[:2])
+    grads = (out.reshape(groups * room, units) for out in outs[2:5])
+    return finish(rx, rc, *grads, *outs[5:])
+
+
 def solution(mesh):
+    groups, parts = mesh.shape["sp"], mesh.shape["tp"]
+    plane = parts == 4 and groups % parts == 0 and groups & (groups - 1) == 0
     return jax.shard_map(
-        shards,
+        plane_shards if plane else shards,
         mesh=mesh,
         in_specs=(
             P("sp", "tp"), P("sp", "tp"), P("sp", None), P("sp", None), P("sp", "tp"),

time: 95.5 us -> 86.6 us (0.907)
  Pallas kernels: 93.4 us -> 85.8 us
  local copies, waits for them, and re-layouts: 1.35 us -> 0 us
    pallas_call x2, Pallas kernels: 93.4 us -> 85.8 us  [the longest x1 80.3 us: plane_shards(): pl.pallas_call(run, out_shape=[jax.ShapeDtypeStruct((groups, room, model)...]
    unnamed x4 -> x0, local copies, waits for them, and re-layouts: 1.35 us -> none
where the time goes in v3:
time: 86.6 us; the launch traced here: 86.4 us
  Pallas kernels  85.8 us (99%)
    pallas_call x1, Pallas kernels, plane_shards(): pl.pallas_call(run, out_shape=[jax.ShapeDtypeStruct((groups, room, model)...  80.3 us
    pallas_call x1, Pallas kernels, finish(): pl.pallas_call(finish_kernel, out_shape=[jax.ShapeDtypeStruct(g, F32) for...  5.54 us

profile of v3, /device:TPU:0, one launch (start us, length us, event | category | flops | bytes accessed | tf_op | source)
XLA Modules:
  0.0 86.4 jit_solution(6457156046545307789)
XLA Ops:
  0.6 80.3 %backward.1 = (bf16[8,40,2048]{2,1,0:T(8,128)(2,1)S(1)}, bf16[8,40,2048]{2,1,0:T(8,128)(2,1)S(1)}, bf16[8,40,512]{2,1,0:T(8,128)(2,1)S(1)}, bf16[8,40,512]{2,1,0...) custom-call(s32[2,128]{1,0:T(2,128)} %bitcast.19, ...), custom_call_target="tpu_custom_call" | custom-call | tf_op jit(solution)/shard_map/backward/pallas_call | solution.py:914
  80.9 5.5 %finish.1 = (f32[2048,512]{1,0:T(8,128)}, f32[2048,512]{1,0:T(8,128)}, f32[512,2048]{1,0:T(8,128)}, f32[256,640]{1,0:T(8,128)}, bf16[128,640]{1,0:T(8,128)(2,1)}...) custom-call(bf16[320,2048]{1,0:T(8,128)(2,1)S(1)} %bitcast.12, bf16[320,2048]{1,0:T(8,128)(2,1)S(1)} %bitcast.13, ...), custom_call_target="tpu_custom_call" | custom-call | tf_op jit(solution)/shard_map/finish/pallas_call | solution.py:416

commit v4 on v3

--- a/solution.py
+++ b/solution.py
@@ -389,19 +389,17 @@
         o = pltpu.make_async_copy(src, dst, small_sems.at[i])
         o.start()
         stores.append(o)
-    steps = sems.shape[1]
-    step = rx.shape[1] // steps
+    step = 256
+    steps = rx.shape[1] // step
     for i in range(steps):
         part = slice(i * step, (i + 1) * step)
         for kind, grad, buf, out in ((0, gpg, gg, gg_out), (1, gpu, gu, gu_out)):
             buf[part, :] = contract_rows(rx[:, part], grad[...])
-            o = pltpu.make_async_copy(buf.at[part], out.at[part], sems.at[kind, i])
-            o.start()
-            stores.append(o)
+            pltpu.make_async_copy(buf.at[part], out.at[part], sems.at[kind]).start()
         gd[:, part] = contract_rows(hid[...], rc[:, part])
-        o = pltpu.make_async_copy(gd.at[:, part], gd_out.at[:, part], sems.at[2, i])
-        o.start()
-        stores.append(o)
+        pltpu.make_async_copy(gd.at[:, part], gd_out.at[:, part], sems.at[2]).start()
+    for kind, (buf, out) in enumerate(((gg, gg_out), (gu, gu_out), (gd, gd_out))):
+        pltpu.make_async_copy(buf, out, sems.at[kind]).wait()
     for o in stores:
         o.wait()
 
@@ -409,7 +407,6 @@
 def finish(rx, rc, hid, gpg, gpu, *small):
     size, model = rx.shape
     units = hid.shape[1]
-    steps = model // 256
     vmem = pl.BlockSpec(memory_space=pltpu.VMEM)
     hbm = pl.BlockSpec(memory_space=pltpu.HBM)
     grads = [(model, units), (model, units), (units, model)]
@@ -420,7 +417,7 @@
         in_specs=[vmem] * (5 + len(small)),
         out_specs=[hbm] * (3 + len(small)),
         scratch_shapes=[pltpu.VMEM(g, F32) for g in grads]
-        + [pltpu.SemaphoreType.DMA((3, steps)), pltpu.SemaphoreType.DMA((len(small),))],
+        + [pltpu.SemaphoreType.DMA((3,)), pltpu.SemaphoreType.DMA((len(small),))],
         compiler_params=pltpu.CompilerParams(vmem_limit_bytes=40 * 1024 * 1024),
         name="finish",
     )(rx, rc, hid, gpg, gpu, *small)
@@ -510,11 +507,9 @@
     rows_x, rows_c, hid_ref, gpg_ref, gpu_ref, outp_ref, ggate_ref, gdecay_ref, gin_ref,
     routes_ref, weights_ref, x_ref, cot_ref, gate_ref, states_ref, decay_ref, wg, wu, wd,
     out_x, out_c, picked_ref, proj_all, mixed_all, act_ref, slope_ref, active_ref, lean_ref,
-    terms, shares, summed, back, cot_turned, cot_mine, flipped, blocks, levels, span_ref, past_ref,
+    terms, shares, passed, summed, back, cot_turned, cot_mine, flipped, blocks, levels, span_ref, past_ref,
     carry_own, carry_in, prev_in,
-    a_send, a_recv, t_send, t_recv, z_send, z_recv, c_send, c_recv,
-    s_send, s_recv, r_send, r_recv, g_send, g_recv, b_send, b_recv, q_send, q_recv, u_send, u_recv,
-    k_send, k_recv, p_send, p_recv, l_sem,
+    o_send, a_recv, t_recv, e_recv, s_recv, m_recv, z_send, z_recv, c_recv, p_send, p_recv, l_sem,
 ):
     mine, col = lax.axis_index("sp"), lax.axis_index("tp")
     toks, width = x_ref.shape
@@ -526,7 +521,7 @@
     size = groups * room
     half = groups // 2
     rows_half = half * room
-    started = []
+    inner = jnp.logical_and(z >= 1, z + 1 < depth)
 
     barrier = pltpu.get_barrier_semaphore()
     for d in range(1, groups):
@@ -557,8 +552,13 @@
     def send(src, dst, send_sem, recv_sem, axis, peer):
         c = remote(src, dst, send_sem, recv_sem, axis, peer)
         c.start()
-        started.append(c)
         return c
+
+    def all_sent(ref, sem):
+        remote(ref, ref, sem, sem, "tp", tile[1]).wait_send()
+
+    def all_here(ref, sem):
+        remote(ref, ref, sem, sem, "tp", tile[1]).wait_recv()
 
     group = [flip(mine, d, groups) for d in range(groups)]
     tile = [flip(col, p, parts) for p in range(parts)]
@@ -576,7 +576,7 @@
         src, dst = sources[a]
         for d in range(1, groups):
             arrivals[a][d] = send(
-                src.at[group[d]], dst.at[mine, :, here], a_send.at[a, d], a_recv.at[a, d], "sp", group[d])
+                src.at[group[d]], dst.at[mine, :, here], o_send.at[a], a_recv.at[a, d - 1], "sp", group[d])
         dst[mine, :, here] = src[mine]
 
     def share_out(a, d):
@@ -585,7 +585,8 @@
             arrivals[a][d].wait_recv()
         own = dst.at[group[d], :, here] if d else src.at[mine]
         gathers[a][d] = [
-            send(own, dst.at[group[d], :, here], t_send.at[a, d, k], t_recv.at[a, d, k], "tp", tile[k + 1])
+            send(own, dst.at[group[d], :, here], o_send.at[2 + a],
+                 t_recv.at[a, d] if k == d % 2 else e_recv.at[a, d // half], "tp", tile[k + 1])
             for k in range(2)
         ]
 
@@ -594,12 +595,10 @@
         k = d % 2
         gathers[a][d][k].wait_recv()
         ref = dst.at[group[d], :, near(width, tile[k + 1])]
-        gathers[a][d].append(
-            send(ref, ref, t_send.at[a, d, 2], t_recv.at[a, d, 2], "tp", tile[2 - k]))
-
-    def landed(a, d):
-        gathers[a][d][1 - d % 2].wait_recv()
-        gathers[a][d][2].wait_recv()
+        send(ref, ref, o_send.at[2 + a], e_recv.at[a, d // half], "tp", tile[2 - k])
+
+    def landed(a, h):
+        all_here(sources[a][1].at[pl.ds(0, groups // parts)], e_recv.at[a, h])
 
     loads[0].wait()
     got = jnp.dot(picked, x_ref[...], preferred_element_type=F32).astype(BF)
@@ -617,16 +616,21 @@
 
     pairs = (proj_all, mixed_all)
 
-    def chain(a, step, wait=False):
+    def chain(a, step, wait=False, middle=None):
         buf = pairs[a]
         right = buf.at[jnp.maximum(z - step, 0) * CORES + core]
         left = buf.at[jnp.minimum(z + step, depth - 1) * CORES + core]
         up = jnp.minimum(z + 1, depth - 1) * CORES + core
         down = jnp.maximum(z - 1, 0) * CORES + core
-        for way, ref, peer, ok in (
-            (0, right, up, jnp.logical_and(z - step >= 0, z + 1 < depth)),
-            (1, left, down, jnp.logical_and(z + step < depth, z >= 1)),
+        for way, ref, peer, ok, within in (
+            (0, right, up, jnp.logical_and(z - step >= 0, z + 1 < depth),
+             jnp.logical_and(z >= 1, z + 2 < depth)),
+            (1, left, down, jnp.logical_and(z + step < depth, z >= 1),
+             jnp.logical_and(z >= 2, z + 1 < depth)),
         ):
+            if middle is not None:
+                ok = jnp.logical_and(ok, within if middle else jnp.logical_not(within))
+
             @pl.when(ok)
             def _(way=way, ref=ref, peer=peer):
                 c = remote(ref, ref, z_send.at[a, way, step], z_recv.at[a, way, step], "sp", peer)
@@ -634,76 +638,90 @@
 
     partner = z * CORES + (1 - core)
 
-    def across(a, step, way, mode):
+    def across(a, step, way, start=True, also=None):
         ok = z - step >= 0 if way == 0 else z + step < depth
+        if also is not None:
+            ok = jnp.logical_and(ok, also)
         zz = jnp.maximum(z - step, 0) if way == 0 else jnp.minimum(z + step, depth - 1)
-        ref = pairs[a].at[zz * CORES + (1 - core if mode == "recv" else core)]
+        ref = pairs[a].at[zz * CORES + (core if start else 1 - core)]
+        sem = c_recv.at[1 + way * depth + step if a else 0]
 
         @pl.when(ok)
         def _():
-            c = remote(ref, ref, c_send.at[a, way, step], c_recv.at[a, way, step], "sp", partner)
-            if mode == "start":
-                c.start()
-            elif mode == "send":
-                c.wait_send()
-            else:
-                c.wait_recv()
-
-    def advance(a, step):
+            c = remote(ref, ref, o_send.at[4 + a], sem, "sp", partner)
+            c.start() if start else c.wait_recv()
+
+    def advance(a, step, also=None):
         buf = pairs[a]
         from_l = buf.at[jnp.maximum(z - 1 - step, 0) * CORES + core]
         from_r = buf.at[jnp.minimum(z + 1 + step, depth - 1) * CORES + core]
         for way, ok, ref in ((0, z - 1 - step >= 0, from_l), (1, z + 1 + step < depth, from_r)):
-            @pl.when(ok)
+            @pl.when(ok if also is None else jnp.logical_and(ok, also))
             def _(way=way, ref=ref):
                 remote(ref, ref, z_send.at[a, way, step], z_recv.at[a, way, step],
                        "sp", lax.rem(mine + 1, groups)).wait_recv()
-        if step + 1 < depth - 1:
-            chain(a, step + 1)
-        across(a, step + 1, 0, "start")
-        across(a, step + 1, 1, "start")
+                if step + 1 < depth - 1:
+                    forward_to = (z + 1 < depth) if way == 0 else (z >= 1)
+                    peer = jnp.minimum(z + 1, depth - 1) if way == 0 else jnp.maximum(z - 1, 0)
+
+                    @pl.when(forward_to)
+                    def _():
+                        remote(ref, ref, z_send.at[a, way, step + 1], z_recv.at[a, way, step + 1],
+                               "sp", peer * CORES + core).start()
+        across(a, step + 1, 0, also=also)
+        across(a, step + 1, 1, also=also)
 
     def settle(a):
         for step in range(depth - 1):
             chain(a, step, True)
-        for step in range(depth):
-            for way in range(2):
-                if step or not way:
-                    across(a, step, way, "send")
-
-    def collected(a):
-        for step in range(depth):
-            for way in range(2):
-                if step or not way:
-                    across(a, step, way, "recv")
+        all_sent(pairs[a].at[pl.ds(0, depth)], o_send.at[4 + a])
+
+    def collected(step):
+        for way in range(2):
+            if step or not way:
+                across(1, step, way, start=False)
 
     loads[4].wait()
     chain(0, 0)
-    across(0, 0, 0, "start")
+    across(0, 0, 0)
+    share_out(1, 0)
+    share_out(0, 1)
     loads[3].wait()
     prev_copy = send(
         states_ref.at[pl.ds(toks - 8, 8)], prev_in, p_send, p_recv, "sp", lax.rem(mine + 1, groups))
 
-    share_out(0, 1)
     loads[2].wait()
     act, branch_slope = gelu_parts(gate_ref[...].astype(F32))
     states = states_ref[...]
     act_ref[...] = act
     slope_ref[...] = branch_slope * states
     mixed_all[mine] = (act * states).astype(BF)
-    for d in range(2, groups):
-        share_out(0, d)
-        relay(0, d - 2)
-    share_out(1, 0)
-    relay(0, groups - 2)
+    chain(1, 0, middle=False)
+    across(1, 0, 0)
     share_out(1, 1)
-    relay(0, groups - 1)
+    share_out(0, 2)
+    share_out(0, 3)
+    for a in range(2):
+        relay(a, 0)
+        relay(a, 1)
+    queue = [(0, d) for d in range(2, groups)] + [(1, d) for d in range(2, groups)]
+    ahead = queue[2:]
+
+    def pump(count):
+        for _ in range(count):
+            for _ in range(2):
+                if ahead:
+                    share_out(*ahead.pop(0))
+            for _ in range(2):
+                if queue:
+                    relay(*queue.pop(0))
+
+    pump(half)
 
     first = [lax.div(mine, half) * half, (1 - lax.div(mine, half)) * half]
 
     def forward(h):
-        for d in range(h * half, (h + 1) * half):
-            landed(0, d)
+        landed(0, h)
         at = pl.ds(first[h], half)
         data = rows_x[at].reshape(rows_half, model)
         pre_gate = jnp.dot(data, wg[...].reshape(model, units), preferred_element_type=F32)
@@ -714,8 +732,7 @@
         lean_ref[h] = pre_up * slope
 
     def hidden_grads(h):
-        for d in range(h * half, (h + 1) * half):
-            landed(1, d)
+        landed(1, h)
         at = pl.ds(first[h], half)
         grad_hidden = contract_cols(rows_c[at].reshape(rows_half, model), wd[...])
         gpg_ref[at] = (grad_hidden * lean_ref[h]).astype(BF).reshape(half, room, units)
@@ -733,28 +750,35 @@
     share_copies = {}
 
     def reduce_out(d):
-        for p in range(1, parts):
-            share_copies[d, p] = send(
-                terms.at[p, group[d]], shares.at[p - 1, group[d]],
-                s_send.at[d, p], s_recv.at[d, p], "tp", tile[p])
-
-    late = list(range(2, groups))
-    waiting = list(range(groups))
-
-    def pump(count):
-        for _ in range(count):
-            if late:
-                share_out(1, late.pop(0))
-            if waiting and (not late or waiting[0] <= late[0] - 3):
-                relay(1, waiting.pop(0))
-
-    pump(2)
+        g, near_tile = group[d], 1 + d % 2
+        share_copies[d] = [
+            send(terms.at[p, g], shares.at[i, g], o_send.at[7], s_recv.at[d, i], "tp", tile[near_tile])
+            for i, p in enumerate((3, near_tile))
+        ]
+
+    def pass_on(d):
+        g, far_tile = group[d], 2 - d % 2
+        share_copies[d][0].wait_recv()
+        passed[g] = (terms[far_tile, g].astype(F32) + shares[0, g].astype(F32)).astype(BF)
+        send(passed.at[g], shares.at[2, g], o_send.at[7], s_recv.at[d, 1], "tp", tile[far_tile])
+
+    def bring_back(d):
+        g = group[d]
+        all_here(shares.at[pl.ds(1, 2), g], s_recv.at[d, 1])
+        total = terms[0, g].astype(F32) + shares[1, g].astype(F32) + shares[2, g].astype(F32)
+        if d == 0:
+            back[mine] = total.astype(BF)
+        else:
+            summed[d] = total.astype(BF)
+            send(summed.at[d], back.at[mine], o_send.at[8], m_recv.at[1], "sp", g)
+
     for i in (6, 7, 8):
         loads[i].wait()
     forward(0)
-    pump(2)
+    pump(1)
+    advance(0, 0)
+    chain(1, 0, middle=True)
     forward(1)
-    pump(2)
 
     rows = lax.broadcasted_iota(jnp.int32, (toks, toks), 0)
     cols = lax.broadcasted_iota(jnp.int32, (toks, toks), 1)
@@ -763,23 +787,24 @@
     cot_turned[...] = contract_rows(cot_ref[...], eye).astype(BF).reshape(cot_turned.shape)
     cot_mine[col] = cot_turned[:, col]
 
-    while len(waiting) > 2:
-        relay(1, waiting.pop(0))
     hidden_grads(0)
-    while waiting:
-        relay(1, waiting.pop(0))
-    cot_copies = [
-        send(cot_turned.at[:, tile[p]], cot_mine.at[col], u_send.at[p], u_recv.at[p], "tp", tile[p])
-        for p in range(1, parts)
-    ]
+    pump(1)
+    for p in range(1, parts):
+        send(cot_turned.at[:, tile[p]], cot_mine.at[col], o_send.at[6], m_recv.at[0], "tp", tile[p])
     input_grads(0)
-    for d in range(1, half):
+    order = list(range(2, half)) + [1, 0] + list(range(half, groups))
+    early = [d for d in order if d < half]
+    for d in early:
         reduce_out(d)
     hidden_grads(1)
+    for d in early[:2]:
+        pass_on(d)
     input_grads(1)
-    for d in list(range(half, groups)) + [0]:
-        reduce_out(d)
-    advance(0, 0)
+    for d in order:
+        if d not in early:
+            reduce_out(d)
+    for d in early[2:]:
+        pass_on(d)
 
     loads[5].wait()
     prev_copy.wait_recv()
@@ -798,51 +823,45 @@
     span_ref[...] = span
     head = decays[0:1]
 
-    for i, d in enumerate(list(range(1, groups)) + [0]):
-        for p in range(1, parts):
-            share_copies[d, p].wait_recv()
-        total = terms[0, group[d]].astype(F32)
-        for p in range(1, parts):
-            total = total + shares[p - 1, group[d]].astype(F32)
-        if d == 0:
-            back[mine] = total.astype(BF)
-        else:
-            summed[d] = total.astype(BF)
-            arrivals[0][d] = send(
-                summed.at[d], back.at[mine], r_send.at[d], r_recv.at[d], "sp", group[d])
-        if i == half:
-            for step in range(1, depth - 1):
-                advance(0, step)
-            chain(1, 0)
-            across(1, 0, 0, "start")
-    advance(1, 0)
-    for c in cot_copies:
-        c.wait_recv()
+    late = [d for d in order if d not in early]
+    for d in order:
+        if late:
+            pass_on(late.pop(0))
+        bring_back(d)
+    for step in range(1, depth - 2):
+        advance(0, step)
+    all_here(cot_turned.at[:, pl.ds(0, parts - 1)], m_recv.at[0])
     total = cot_mine[...].reshape(width, toks).astype(F32)
-    for d in range(1, groups):
-        arrivals[0][d].wait_recv()
+    all_here(back.at[pl.ds(0, groups - 1)], m_recv.at[1])
     total = total + contract_rows(back[...].reshape(size, width), picked_ref[...])
     flipped[:, col] = total.astype(BF).reshape(groups, fine, toks)
-    grad_copies = []
-    for p in range(1, parts):
-        part = flipped.at[:, col]
-        grad_copies.append(send(part, part, g_send.at[p], g_recv.at[p], "tp", tile[p]))
-    block_copies = [
-        send(flipped.at[group[d], col], blocks.at[mine, col], b_send.at[d], b_recv.at[d], "sp", group[d])
-        for d in range(1, groups)
-    ]
+
+    def plane_start(buf, first_sem):
+        part = buf.at[:, col]
+        return [
+            send(part, part, o_send.at[first_sem // 3 + 8], m_recv.at[first_sem + p], "tp", tile[p])
+            for p in (1, 2)
+        ]
+
+    def plane_relay(buf, copies, first_sem):
+        for p in (1, 2):
+            copies[p - 1].wait_recv()
+            part = buf.at[pl.ds((p - 1) * half, half), tile[p]]
+            send(part, part, o_send.at[first_sem // 3 + 8], m_recv.at[first_sem], "tp", tile[3 - p])
+
+    grad_copies = plane_start(flipped, 3)
+    for d in range(1, groups):
+        send(flipped.at[group[d], col], blocks.at[mine, col], o_send.at[11], m_recv.at[2], "sp", group[d])
     blocks[mine, col] = flipped[mine, col]
-    for step in range(1, depth - 1):
-        advance(1, step)
-    for c in block_copies:
-        c.wait_recv()
-    plane_copies = []
-    for p in range(1, parts):
-        part = blocks.at[:, col]
-        plane_copies.append(send(part, part, q_send.at[p], q_recv.at[p], "tp", tile[p]))
-    collected(0)
-    for c in grad_copies:
-        c.wait_recv()
+    advance(1, 0)
+    plane_relay(flipped, grad_copies, 3)
+    all_here(blocks.at[pl.ds(0, groups - 1), 0], m_recv.at[2])
+    plane_copies = plane_start(blocks, 6)
+    advance(0, depth - 2)
+    for step in range(1, depth - 2):
+        advance(1, step, inner)
+    all_here(flipped.at[:, 0], m_recv.at[3])
+    all_here(proj_all.at[pl.ds(0, depth)], c_recv.at[0])
     grad_mixed = contract_rows(flipped[...].reshape(model, toks), proj_all[...].reshape(model, chans))
     ggate_ref[...] = (grad_mixed * slope_ref[...]).astype(BF)
     local = grad_mixed * act_ref[...]
@@ -853,22 +872,24 @@
         level += 1
     eight = lax.broadcasted_iota(jnp.int32, (8, chans), 0)
     carry_own[...] = jnp.where(eight == 0, span_ref[0:1, :] * head, local[0:1] * head)
-    carry_copies = []
     for d in range(1, groups):
-        peer = lax.rem(mine + d, groups)
-        carry_copies.append(
-            send(carry_own, carry_in.at[d - 1], k_send.at[d], k_recv.at[d], "sp", peer))
-    collected(1)
-    for c in plane_copies:
-        c.wait_recv()
+        send(carry_own, carry_in.at[d - 1], o_send.at[12], m_recv.at[9], "sp", lax.rem(mine + d, groups))
+    plane_relay(blocks, plane_copies, 6)
+    for step in range(1, depth - 2):
+        advance(1, step, jnp.logical_not(inner))
+    for step in range(depth - 1):
+        collected(step)
+    all_here(blocks.at[:, 0], m_recv.at[6])
     high = blocks.shape[1] * blocks.shape[2]
-    total = jnp.zeros((high, chans), F32)
-    for t in range(groups):
-        total = total + jnp.dot(
-            blocks[t].reshape(high, toks), mixed_all[t], preferred_element_type=F32)
-    outp_ref[...] = total
-    for c in carry_copies:
-        c.wait_recv()
+
+    def out_part(t):
+        return jnp.dot(blocks[t].reshape(high, toks), mixed_all[t], preferred_element_type=F32)
+
+    near_part = out_part(group[0])
+    for d in range(1, groups - CORES):
+        near_part = near_part + out_part(group[d])
+    outp_ref[...] = near_part
+    all_here(carry_in, m_recv.at[9])
     carried = jnp.zeros((1, chans), F32)
     for ahead in range(groups - 1, 0, -1):
         got = carry_in[groups - ahead - 1]
@@ -876,10 +897,25 @@
     grad_in = local + span_ref[...] * carried
     gin_ref[...] = grad_in
     gdecay_ref[...] = (grad_in * past_ref[...]).astype(BF)
+    advance(1, depth - 2)
+    collected(depth - 1)
+    far_part = out_part(group[groups - CORES])
+    for d in range(groups - CORES + 1, groups):
+        far_part = far_part + out_part(group[d])
+    outp_ref[...] += far_part
     settle(0)
     settle(1)
-    for c in started:
-        c.wait_send()
+    for a in range(2):
+        all_sent(rows_x.at[pl.ds(0, groups - 1), :, pl.ds(0, width)], o_send.at[a])
+        all_sent(rows_x.at[pl.ds(0, groups * 3 // parts)], o_send.at[2 + a])
+    all_sent(cot_turned.at[:, pl.ds(0, parts - 1)], o_send.at[6])
+    all_sent(rows_x.at[pl.ds(0, groups * 3 // parts)], o_send.at[7])
+    all_sent(back.at[pl.ds(0, groups - 1)], o_send.at[8])
+    for i in (9, 10):
+        all_sent(flipped.at[:, pl.ds(0, 3)], o_send.at[i])
+    all_sent(blocks.at[pl.ds(0, groups - 1), 0], o_send.at[11])
+    all_sent(carry_in, o_send.at[12])
+    prev_copy.wait_send()
 
 
 def plane_shards(
@@ -936,17 +972,16 @@
             buf(tok_rows, chans, kind=F32), buf(tok_rows, chans, kind=F32),
             buf(2, groups // 2 * room, units, kind=F32), buf(2, groups // 2 * room, units, kind=F32),
             buf(parts, groups, room, width), buf(parts - 1, groups, room, width),
-            buf(groups, room, width), buf(groups, room, width),
+            buf(groups, room, width), buf(groups, room, width), buf(groups, room, width),
             buf(groups // parts, parts, fine, tok_rows), buf(parts, groups // parts, fine, tok_rows),
             buf(groups, parts, fine, tok_rows), buf(groups, parts, fine, tok_rows),
             buf(doublings, tok_rows, chans, kind=F32), buf(tok_rows, chans, kind=F32),
             buf(tok_rows, chans, kind=F32),
             buf(8, chans, kind=F32), buf(groups - 1, 8, chans, kind=F32), buf(8, chans, kind=F32),
         ]
-        + [dma((2, groups))] * 2 + [dma((2, groups, 3))] * 2 + [dma((2, 2, depth))] * 4
-        + [dma((groups, parts))] * 2 + [dma((groups,))] * 2 + [dma((parts,))] * 2
-        + [dma((groups,))] * 2 + [dma((parts,))] * 4
-        + [dma((groups,))] * 2 + [dma(())] * 2 + [dma((11,))],
+        + [dma((13,)), dma((2, groups - 1)), dma((2, groups)), dma((2, 2)), dma((groups, 2))]
+        + [dma((10,)), dma((2, 2, depth - 1)), dma((2, 2, depth - 1)), dma((1 + 2 * depth,))]
+        + [dma(()), dma(()), dma((11,))],
         compiler_params=pltpu.CompilerParams(
             collective_id=0, has_side_effects=True, vmem_limit_bytes=40 * 1024 * 1024),
         name="backward",

time: 86.6 us -> 75.9 us (0.88)
  Pallas kernels: 85.8 us -> 75.1 us
    pallas_call x1, Pallas kernels: 80.3 us -> 69.7 us  [plane_shards(): pl.pallas_call(run, out_shape=[jax.ShapeDtypeStruct((groups, room, model)...]
where the time goes in v4:
time: 75.9 us; the launch traced here: 75.7 us
  Pallas kernels  75.1 us (99%)
    pallas_call x1, Pallas kernels, plane_shards(): pl.pallas_call(run, out_shape=[jax.ShapeDtypeStruct((groups, room, model)...  69.7 us
    pallas_call x1, Pallas kernels, finish(): pl.pallas_call(finish_kernel, out_shape=[jax.ShapeDtypeStruct(g, F32) for...  5.35 us

profile of v4, /device:TPU:0, one launch (start us, length us, event | category | flops | bytes accessed | tf_op | source)
XLA Modules:
  0.0 75.7 jit_solution(3984074975243476194)
XLA Ops:
  0.6 69.7 %backward.1 = (bf16[8,40,2048]{2,1,0:T(8,128)(2,1)S(1)}, bf16[8,40,2048]{2,1,0:T(8,128)(2,1)S(1)}, bf16[8,40,512]{2,1,0:T(8,128)(2,1)S(1)}, bf16[8,40,512]{2,1,0...) custom-call(s32[2,128]{1,0:T(2,128)} %bitcast.19, ...), custom_call_target="tpu_custom_call" | custom-call | tf_op jit(solution)/shard_map/backward/pallas_call | solution.py:950
  70.4 5.4 %finish.1 = (f32[2048,512]{1,0:T(8,128)}, f32[2048,512]{1,0:T(8,128)}, f32[512,2048]{1,0:T(8,128)}, f32[256,640]{1,0:T(8,128)}, bf16[128,640]{1,0:T(8,128)(2,1)}...) custom-call(bf16[320,2048]{1,0:T(8,128)(2,1)S(1)} %bitcast.12, bf16[320,2048]{1,0:T(8,128)(2,1)S(1)} %bitcast.13, ...), custom_call_target="tpu_custom_call" | custom-call | tf_op jit(solution)/shard_map/finish/pallas_call | solution.py:413

commit v5 on v4

--- a/solution.py
+++ b/solution.py
@@ -614,7 +614,10 @@
         out_c[e] = got[e * room : (e + 1) * room]
     spread(1)
 
-    pairs = (proj_all, mixed_all)
+    low = proj_all.shape[1] // 2
+    pairs = (proj_all.at[:, pl.ds(0, low)], proj_all.at[:, pl.ds(low, low)], mixed_all)
+    last = len(pairs) - 1
+    hop_send = (4, 13, 5)
 
     def chain(a, step, wait=False, middle=None):
         buf = pairs[a]
@@ -644,11 +647,11 @@
             ok = jnp.logical_and(ok, also)
         zz = jnp.maximum(z - step, 0) if way == 0 else jnp.minimum(z + step, depth - 1)
         ref = pairs[a].at[zz * CORES + (core if start else 1 - core)]
-        sem = c_recv.at[1 + way * depth + step if a else 0]
+        sem = c_recv.at[last + way * depth + step if a == last else a]
 
         @pl.when(ok)
         def _():
-            c = remote(ref, ref, o_send.at[4 + a], sem, "sp", partner)
+            c = remote(ref, ref, o_send.at[hop_send[a]], sem, "sp", partner)
             c.start() if start else c.wait_recv()
 
     def advance(a, step, also=None):
@@ -674,16 +677,17 @@
     def settle(a):
         for step in range(depth - 1):
             chain(a, step, True)
-        all_sent(pairs[a].at[pl.ds(0, depth)], o_send.at[4 + a])
+        all_sent(pairs[a].at[pl.ds(0, depth)], o_send.at[hop_send[a]])
 
     def collected(step):
         for way in range(2):
             if step or not way:
-                across(1, step, way, start=False)
+                across(last, step, way, start=False)
 
     loads[4].wait()
-    chain(0, 0)
-    across(0, 0, 0)
+    for a in range(last):
+        chain(a, 0)
+        across(a, 0, 0)
     share_out(1, 0)
     share_out(0, 1)
     loads[3].wait()
@@ -696,9 +700,17 @@
     act_ref[...] = act
     slope_ref[...] = branch_slope * states
     mixed_all[mine] = (act * states).astype(BF)
-    chain(1, 0, middle=False)
-    across(1, 0, 0)
+    chain(last, 0, middle=False)
+    across(last, 0, 0)
+    rows = lax.broadcasted_iota(jnp.int32, (toks, toks), 0)
+    cols = lax.broadcasted_iota(jnp.int32, (toks, toks), 1)
+    eye = jnp.where(rows == cols, 1.0, 0.0).astype(BF)
+    fine = cot_turned.shape[2]
+    cot_turned[...] = contract_rows(cot_ref[...], eye).astype(BF).reshape(cot_turned.shape)
+    cot_mine[col] = cot_turned[:, col]
     share_out(1, 1)
+    for p in range(1, parts):
+        send(cot_turned.at[:, tile[p]], cot_mine.at[col], o_send.at[6], m_recv.at[0], "tp", tile[p])
     share_out(0, 2)
     share_out(0, 3)
     for a in range(2):
@@ -738,23 +750,26 @@
         gpg_ref[at] = (grad_hidden * lean_ref[h]).astype(BF).reshape(half, room, units)
         gpu_ref[at] = (grad_hidden * active_ref[h]).astype(BF).reshape(half, room, units)
 
-    def input_grads(h):
+    share_copies = [[None, None] for _ in range(groups)]
+
+    def reduce_out(d, i, p):
+        g = group[d]
+        share_copies[d][i] = send(
+            terms.at[p, g], shares.at[i, g], o_send.at[7], s_recv.at[d, i], "tp", tile[1 + d % 2])
+
+    def input_grads(h, order):
         at = pl.ds(first[h], half)
         gate_part = gpg_ref[at].reshape(rows_half, units)
         up_part = gpu_ref[at].reshape(rows_half, units)
-        for p in list(range(1, parts)) + [0]:
+        for p in (3, 1, 2, 0):
             term = contract_cols(gate_part, wg[:, tile[p]].reshape(width, units))
             term = term + contract_cols(up_part, wu[:, tile[p]].reshape(width, units))
             terms[p, at] = term.astype(BF).reshape(half, room, width)
-
-    share_copies = {}
-
-    def reduce_out(d):
-        g, near_tile = group[d], 1 + d % 2
-        share_copies[d] = [
-            send(terms.at[p, g], shares.at[i, g], o_send.at[7], s_recv.at[d, i], "tp", tile[near_tile])
-            for i, p in enumerate((3, near_tile))
-        ]
+            for d in order:
+                if p == 3:
+                    reduce_out(d, 0, p)
+                elif p == 1 + d % 2:
+                    reduce_out(d, 1, p)
 
     def pass_on(d):
         g, far_tile = group[d], 2 - d % 2
@@ -776,34 +791,20 @@
         loads[i].wait()
     forward(0)
     pump(1)
-    advance(0, 0)
-    chain(1, 0, middle=True)
+    for a in range(last):
+        advance(a, 0)
+    chain(last, 0, middle=True)
     forward(1)
-
-    rows = lax.broadcasted_iota(jnp.int32, (toks, toks), 0)
-    cols = lax.broadcasted_iota(jnp.int32, (toks, toks), 1)
-    eye = jnp.where(rows == cols, 1.0, 0.0).astype(BF)
-    fine = cot_turned.shape[2]
-    cot_turned[...] = contract_rows(cot_ref[...], eye).astype(BF).reshape(cot_turned.shape)
-    cot_mine[col] = cot_turned[:, col]
 
     hidden_grads(0)
     pump(1)
-    for p in range(1, parts):
-        send(cot_turned.at[:, tile[p]], cot_mine.at[col], o_send.at[6], m_recv.at[0], "tp", tile[p])
-    input_grads(0)
     order = list(range(2, half)) + [1, 0] + list(range(half, groups))
-    early = [d for d in order if d < half]
-    for d in early:
-        reduce_out(d)
+    input_grads(0, order[:half])
     hidden_grads(1)
-    for d in early[:2]:
+    for d in order[:2]:
         pass_on(d)
-    input_grads(1)
-    for d in order:
-        if d not in early:
-            reduce_out(d)
-    for d in early[2:]:
+    input_grads(1, order[half:])
+    for d in order[2:half]:
         pass_on(d)
 
     loads[5].wait()
@@ -823,45 +824,52 @@
     span_ref[...] = span
     head = decays[0:1]
 
-    late = [d for d in order if d not in early]
+    for step in range(1, depth - 2):
+        advance(0, step)
+    late = order[half:]
     for d in order:
         if late:
             pass_on(late.pop(0))
         bring_back(d)
-    for step in range(1, depth - 2):
-        advance(0, step)
     all_here(cot_turned.at[:, pl.ds(0, parts - 1)], m_recv.at[0])
     total = cot_mine[...].reshape(width, toks).astype(F32)
     all_here(back.at[pl.ds(0, groups - 1)], m_recv.at[1])
     total = total + contract_rows(back[...].reshape(size, width), picked_ref[...])
     flipped[:, col] = total.astype(BF).reshape(groups, fine, toks)
 
+    def plane_part(buf, owner, rows, first_sem, to, relayed=0):
+        part = buf.at[pl.ds(rows * half, half), owner]
+        return send(
+            part, part, o_send.at[first_sem // 3 + 8], m_recv.at[first_sem + relayed], "tp", tile[to])
+
     def plane_start(buf, first_sem):
-        part = buf.at[:, col]
-        return [
-            send(part, part, o_send.at[first_sem // 3 + 8], m_recv.at[first_sem + p], "tp", tile[p])
-            for p in (1, 2)
-        ]
+        copies = [plane_part(buf, col, p - 1, first_sem, p, p) for p in (1, 2)]
+        for p in (1, 2):
+            plane_part(buf, col, 2 - p, first_sem, p)
+        return copies
 
     def plane_relay(buf, copies, first_sem):
         for p in (1, 2):
             copies[p - 1].wait_recv()
-            part = buf.at[pl.ds((p - 1) * half, half), tile[p]]
-            send(part, part, o_send.at[first_sem // 3 + 8], m_recv.at[first_sem], "tp", tile[3 - p])
+            plane_part(buf, tile[p], p - 1, first_sem, 3 - p)
 
     grad_copies = plane_start(flipped, 3)
     for d in range(1, groups):
         send(flipped.at[group[d], col], blocks.at[mine, col], o_send.at[11], m_recv.at[2], "sp", group[d])
     blocks[mine, col] = flipped[mine, col]
-    advance(1, 0)
+    for step in range(1, depth - 2):
+        advance(1, step)
+    advance(last, 0)
     plane_relay(flipped, grad_copies, 3)
     all_here(blocks.at[pl.ds(0, groups - 1), 0], m_recv.at[2])
     plane_copies = plane_start(blocks, 6)
     advance(0, depth - 2)
     for step in range(1, depth - 2):
-        advance(1, step, inner)
-    all_here(flipped.at[:, 0], m_recv.at[3])
-    all_here(proj_all.at[pl.ds(0, depth)], c_recv.at[0])
+        advance(last, step, inner)
+    all_here(flipped.at[:, pl.ds(0, 2)], m_recv.at[3])
+    advance(1, depth - 2)
+    for a in range(last):
+        all_here(pairs[a].at[pl.ds(0, depth)], c_recv.at[a])
     grad_mixed = contract_rows(flipped[...].reshape(model, toks), proj_all[...].reshape(model, chans))
     ggate_ref[...] = (grad_mixed * slope_ref[...]).astype(BF)
     local = grad_mixed * act_ref[...]
@@ -870,16 +878,17 @@
         local = local + levels[level] * pltpu.roll(local, toks - k, 0)
         k *= 2
         level += 1
-    eight = lax.broadcasted_iota(jnp.int32, (8, chans), 0)
-    carry_own[...] = jnp.where(eight == 0, span_ref[0:1, :] * head, local[0:1] * head)
+    carry_own[0:1] = span_ref[0:1, :] * head
+    carry_own[1:2] = local[0:1] * head
     for d in range(1, groups):
         send(carry_own, carry_in.at[d - 1], o_send.at[12], m_recv.at[9], "sp", lax.rem(mine + d, groups))
     plane_relay(blocks, plane_copies, 6)
     for step in range(1, depth - 2):
-        advance(1, step, jnp.logical_not(inner))
+        advance(last, step, jnp.logical_not(inner))
     for step in range(depth - 1):
         collected(step)
-    all_here(blocks.at[:, 0], m_recv.at[6])
+    all_here(blocks.at[:, pl.ds(0, 2)], m_recv.at[6])
+    advance(last, depth - 2)
     high = blocks.shape[1] * blocks.shape[2]
 
     def out_part(t):
@@ -897,14 +906,13 @@
     grad_in = local + span_ref[...] * carried
     gin_ref[...] = grad_in
     gdecay_ref[...] = (grad_in * past_ref[...]).astype(BF)
-    advance(1, depth - 2)
     collected(depth - 1)
     far_part = out_part(group[groups - CORES])
     for d in range(groups - CORES + 1, groups):
         far_part = far_part + out_part(group[d])
     outp_ref[...] += far_part
-    settle(0)
-    settle(1)
+    for a in range(last + 1):
+        settle(a)
     for a in range(2):
         all_sent(rows_x.at[pl.ds(0, groups - 1), :, pl.ds(0, width)], o_send.at[a])
         all_sent(rows_x.at[pl.ds(0, groups * 3 // parts)], o_send.at[2 + a])
@@ -977,10 +985,10 @@
             buf(groups, parts, fine, tok_rows), buf(groups, parts, fine, tok_rows),
             buf(doublings, tok_rows, chans, kind=F32), buf(tok_rows, chans, kind=F32),
             buf(tok_rows, chans, kind=F32),
-            buf(8, chans, kind=F32), buf(groups - 1, 8, chans, kind=F32), buf(8, chans, kind=F32),
+            buf(2, chans, kind=F32), buf(groups - 1, 2, chans, kind=F32), buf(8, chans, kind=F32),
         ]
-        + [dma((13,)), dma((2, groups - 1)), dma((2, groups)), dma((2, 2)), dma((groups, 2))]
-        + [dma((10,)), dma((2, 2, depth - 1)), dma((2, 2, depth - 1)), dma((1 + 2 * depth,))]
+        + [dma((14,)), dma((2, groups - 1)), dma((2, groups)), dma((2, 2)), dma((groups, 2))]
+        + [dma((10,)), dma((3, 2, depth - 1)), dma((3, 2, depth - 1)), dma((2 + 2 * depth,))]
         + [dma(()), dma(()), dma((11,))],
         compiler_params=pltpu.CompilerParams(
             collective_id=0, has_side_effects=True, vmem_limit_bytes=40 * 1024 * 1024),

time: 75.9 us -> 72.7 us (0.958)
  Pallas kernels: 75.1 us -> 71.8 us
    pallas_call x1, Pallas kernels: 69.7 us -> 66.4 us  [plane_shards(): pl.pallas_call(run, out_shape=[jax.ShapeDtypeStruct((groups, room, model)...]
where the time goes in v5:
time: 72.7 us; the launch traced here: 72.4 us
  Pallas kernels  71.8 us (99%)
    pallas_call x1, Pallas kernels, plane_shards(): pl.pallas_call(run, out_shape=[jax.ShapeDtypeStruct((groups, room, model)...  66.4 us
    pallas_call x1, Pallas kernels, finish(): pl.pallas_call(finish_kernel, out_shape=[jax.ShapeDtypeStruct(g, F32) for...  5.36 us

profile of v5, /device:TPU:0, one launch (start us, length us, event | category | flops | bytes accessed | tf_op | source)
XLA Modules:
  0.0 72.4 jit_solution(1527545094529406302)
XLA Ops:
  0.6 66.4 %backward.1 = (bf16[8,40,2048]{2,1,0:T(8,128)(2,1)S(1)}, bf16[8,40,2048]{2,1,0:T(8,128)(2,1)S(1)}, bf16[8,40,512]{2,1,0:T(8,128)(2,1)S(1)}, bf16[8,40,512]{2,1,0...) custom-call(s32[2,128]{1,0:T(2,128)} %bitcast.19, ...), custom_call_target="tpu_custom_call" | custom-call | tf_op jit(solution)/shard_map/backward/pallas_call | solution.py:958
  67.0 5.4 %finish.1 = (f32[2048,512]{1,0:T(8,128)}, f32[2048,512]{1,0:T(8,128)}, f32[512,2048]{1,0:T(8,128)}, f32[256,640]{1,0:T(8,128)}, bf16[128,640]{1,0:T(8,128)(2,1)}...) custom-call(bf16[320,2048]{1,0:T(8,128)(2,1)S(1)} %bitcast.12, bf16[320,2048]{1,0:T(8,128)(2,1)S(1)} %bitcast.13, ...), custom_call_target="tpu_custom_call" | custom-call | tf_op jit(solution)/shard_map/finish/pallas_call | solution.py:413

commit v6 on v5

--- a/solution.py
+++ b/solution.py
@@ -391,13 +391,17 @@
         stores.append(o)
     step = 256
     steps = rx.shape[1] // step
+    units = hid.shape[1]
+    down = units // 4
     for i in range(steps):
         part = slice(i * step, (i + 1) * step)
         for kind, grad, buf, out in ((0, gpg, gg, gg_out), (1, gpu, gu, gu_out)):
             buf[part, :] = contract_rows(rx[:, part], grad[...])
             pltpu.make_async_copy(buf.at[part], out.at[part], sems.at[kind]).start()
-        gd[:, part] = contract_rows(hid[...], rc[:, part])
-        pltpu.make_async_copy(gd.at[:, part], gd_out.at[:, part], sems.at[2]).start()
+        if i % (steps // 4) == 0:
+            rows = slice(i * 4 // steps * down, (i * 4 // steps + 1) * down)
+            gd[rows, :] = contract_rows(hid[:, rows], rc[...])
+            pltpu.make_async_copy(gd.at[rows], gd_out.at[rows], sems.at[2]).start()
     for kind, (buf, out) in enumerate(((gg, gg_out), (gu, gu_out), (gd, gd_out))):
         pltpu.make_async_copy(buf, out, sems.at[kind]).wait()
     for o in stores:
@@ -614,8 +618,9 @@
         out_c[e] = got[e * room : (e + 1) * room]
     spread(1)
 
-    low = proj_all.shape[1] // 2
-    pairs = (proj_all.at[:, pl.ds(0, low)], proj_all.at[:, pl.ds(low, low)], mixed_all)
+    low = proj_all.shape[1] * 3 // 4
+    pairs = (
+        proj_all.at[:, pl.ds(0, low)], proj_all.at[:, pl.ds(low, proj_all.shape[1] - low)], mixed_all)
     last = len(pairs) - 1
     hop_send = (4, 13, 5)
 
@@ -654,25 +659,32 @@
             c = remote(ref, ref, o_send.at[hop_send[a]], sem, "sp", partner)
             c.start() if start else c.wait_recv()
 
-    def advance(a, step, also=None):
-        buf = pairs[a]
-        from_l = buf.at[jnp.maximum(z - 1 - step, 0) * CORES + core]
-        from_r = buf.at[jnp.minimum(z + 1 + step, depth - 1) * CORES + core]
-        for way, ok, ref in ((0, z - 1 - step >= 0, from_l), (1, z + 1 + step < depth, from_r)):
-            @pl.when(ok if also is None else jnp.logical_and(ok, also))
-            def _(way=way, ref=ref):
+    def advance(a, step, also=None, middle=None):
+        for way in range(2):
+            if way == 0:
+                ok, origin, to = z - 1 - step >= 0, jnp.maximum(z - 1 - step, 0), z + 1
+                goes_on, within = z + 1 < depth, jnp.logical_and(z >= 1, z + 2 < depth)
+            else:
+                ok, origin, to = z + 1 + step < depth, jnp.minimum(z + 1 + step, depth - 1), z - 1
+                goes_on, within = z >= 1, jnp.logical_and(z >= 2, z + 1 < depth)
+            ref = pairs[a].at[origin * CORES + core]
+            peer = jnp.clip(to, 0, depth - 1) * CORES + core
+            if also is not None:
+                ok = jnp.logical_and(ok, also)
+            if middle is not None:
+                ok = jnp.logical_and(ok, within if middle else jnp.logical_not(within))
+
+            @pl.when(ok)
+            def _(way=way, ref=ref, peer=peer, goes_on=goes_on):
                 remote(ref, ref, z_send.at[a, way, step], z_recv.at[a, way, step],
                        "sp", lax.rem(mine + 1, groups)).wait_recv()
                 if step + 1 < depth - 1:
-                    forward_to = (z + 1 < depth) if way == 0 else (z >= 1)
-                    peer = jnp.minimum(z + 1, depth - 1) if way == 0 else jnp.maximum(z - 1, 0)
-
-                    @pl.when(forward_to)
+                    @pl.when(goes_on)
                     def _():
                         remote(ref, ref, z_send.at[a, way, step + 1], z_recv.at[a, way, step + 1],
-                               "sp", peer * CORES + core).start()
-        across(a, step + 1, 0, also=also)
-        across(a, step + 1, 1, also=also)
+                               "sp", peer).start()
+
+            across(a, step + 1, way, also=ok)
 
     def settle(a):
         for step in range(depth - 1):
@@ -790,9 +802,9 @@
     for i in (6, 7, 8):
         loads[i].wait()
     forward(0)
+    advance(0, 0)
     pump(1)
-    for a in range(last):
-        advance(a, 0)
+    advance(1, 0)
     chain(last, 0, middle=True)
     forward(1)
 
@@ -831,6 +843,7 @@
         if late:
             pass_on(late.pop(0))
         bring_back(d)
+    advance(last, 0, middle=True)
     all_here(cot_turned.at[:, pl.ds(0, parts - 1)], m_recv.at[0])
     total = cot_mine[...].reshape(width, toks).astype(F32)
     all_here(back.at[pl.ds(0, groups - 1)], m_recv.at[1])
@@ -859,7 +872,7 @@
     blocks[mine, col] = flipped[mine, col]
     for step in range(1, depth - 2):
         advance(1, step)
-    advance(last, 0)
+    advance(last, 0, middle=False)
     plane_relay(flipped, grad_copies, 3)
     all_here(blocks.at[pl.ds(0, groups - 1), 0], m_recv.at[2])
     plane_copies = plane_start(blocks, 6)

time: 72.7 us -> 71.5 us (0.983)
  Pallas kernels: 71.8 us -> 70.6 us
    pallas_call x1, Pallas kernels: 66.4 us -> 65.3 us  [plane_shards(): pl.pallas_call(run, out_shape=[jax.ShapeDtypeStruct((groups, room, model)...]
where the time goes in v6:
time: 71.5 us; the launch traced here: 71.3 us
  Pallas kernels  70.6 us (99%)
    pallas_call x1, Pallas kernels, plane_shards(): pl.pallas_call(run, out_shape=[jax.ShapeDtypeStruct((groups, room, model)...  65.3 us
    pallas_call x1, Pallas kernels, finish(): pl.pallas_call(finish_kernel, out_shape=[jax.ShapeDtypeStruct(g, F32) for...  5.39 us

profile of v6, /device:TPU:0, one launch (start us, length us, event | category | flops | bytes accessed | tf_op | source)
XLA Modules:
  0.0 71.3 jit_solution(6375252387328849938)
XLA Ops:
  0.6 65.3 %backward.1 = (bf16[8,40,2048]{2,1,0:T(8,128)(2,1)S(1)}, bf16[8,40,2048]{2,1,0:T(8,128)(2,1)S(1)}, bf16[8,40,512]{2,1,0:T(8,128)(2,1)S(1)}, bf16[8,40,512]{2,1,0...) custom-call(s32[2,128]{1,0:T(2,128)} %bitcast.19, ...), custom_call_target="tpu_custom_call" | custom-call | tf_op jit(solution)/shard_map/backward/pallas_call | solution.py:971
  65.9 5.4 %finish.1 = (f32[2048,512]{1,0:T(8,128)}, f32[2048,512]{1,0:T(8,128)}, f32[512,2048]{1,0:T(8,128)}, f32[256,640]{1,0:T(8,128)}, bf16[128,640]{1,0:T(8,128)(2,1)}...) custom-call(bf16[320,2048]{1,0:T(8,128)(2,1)S(1)} %bitcast.12, bf16[320,2048]{1,0:T(8,128)(2,1)S(1)} %bitcast.13, ...), custom_call_target="tpu_custom_call" | custom-call | tf_op jit(solution)/shard_map/finish/pallas_call | solution.py:417

commit v7 on v6

--- a/solution.py
+++ b/solution.py
@@ -624,7 +624,7 @@
     last = len(pairs) - 1
     hop_send = (4, 13, 5)
 
-    def chain(a, step, wait=False, middle=None):
+    def chain(a, step, middle=None):
         buf = pairs[a]
         right = buf.at[jnp.maximum(z - step, 0) * CORES + core]
         left = buf.at[jnp.minimum(z + step, depth - 1) * CORES + core]
@@ -641,8 +641,8 @@
 
             @pl.when(ok)
             def _(way=way, ref=ref, peer=peer):
-                c = remote(ref, ref, z_send.at[a, way, step], z_recv.at[a, way, step], "sp", peer)
-                c.wait_send() if wait else c.start()
+                c = remote(ref, ref, z_send.at[a], z_recv.at[a, way, step], "sp", peer)
+                c.start()
 
     partner = z * CORES + (1 - core)
 
@@ -676,19 +676,25 @@
 
             @pl.when(ok)
             def _(way=way, ref=ref, peer=peer, goes_on=goes_on):
-                remote(ref, ref, z_send.at[a, way, step], z_recv.at[a, way, step],
+                remote(ref, ref, z_send.at[a], z_recv.at[a, way, step],
                        "sp", lax.rem(mine + 1, groups)).wait_recv()
                 if step + 1 < depth - 1:
                     @pl.when(goes_on)
                     def _():
-                        remote(ref, ref, z_send.at[a, way, step + 1], z_recv.at[a, way, step + 1],
+                        remote(ref, ref, z_send.at[a], z_recv.at[a, way, step + 1],
                                "sp", peer).start()
 
             across(a, step + 1, way, also=ok)
 
     def settle(a):
-        for step in range(depth - 1):
-            chain(a, step, True)
+        for at in range(depth):
+            hops = (min(at + 1, depth - 1) if at + 1 < depth else 0) + (
+                min(depth - at, depth - 1) if at else 0)
+
+            @pl.when(z == at)
+            def _(hops=hops):
+                all_sent(pairs[a].at[pl.ds(0, hops)], z_send.at[a])
+
         all_sent(pairs[a].at[pl.ds(0, depth)], o_send.at[hop_send[a]])
 
     def collected(step):
@@ -1001,7 +1007,7 @@
             buf(2, chans, kind=F32), buf(groups - 1, 2, chans, kind=F32), buf(8, chans, kind=F32),
         ]
         + [dma((14,)), dma((2, groups - 1)), dma((2, groups)), dma((2, 2)), dma((groups, 2))]
-        + [dma((10,)), dma((3, 2, depth - 1)), dma((3, 2, depth - 1)), dma((2 + 2 * depth,))]
+        + [dma((10,)), dma((3,)), dma((3, 2, depth - 1)), dma((2 + 2 * depth,))]
         + [dma(()), dma(()), dma((11,))],
         compiler_params=pltpu.CompilerParams(
             collective_id=0, has_side_effects=True, vmem_limit_bytes=40 * 1024 * 1024),

time: 71.5 us -> 71.3 us (level)
  no operation moved by 1% of the time
where the time goes in v7:
time: 71.3 us; the launch traced here: 71.2 us
  Pallas kernels  70.5 us (99%)
    pallas_call x1, Pallas kernels, plane_shards(): pl.pallas_call(run, out_shape=[jax.ShapeDtypeStruct((groups, room, model)...  65.1 us
    pallas_call x1, Pallas kernels, finish(): pl.pallas_call(finish_kernel, out_shape=[jax.ShapeDtypeStruct(g, F32) for...  5.39 us

profile of v7, /device:TPU:0, one launch (start us, length us, event | category | flops | bytes accessed | tf_op | source)
XLA Modules:
  0.0 71.2 jit_solution(3456879077455271594)
XLA Ops:
  0.6 65.1 %backward.1 = (bf16[8,40,2048]{2,1,0:T(8,128)(2,1)S(1)}, bf16[8,40,2048]{2,1,0:T(8,128)(2,1)S(1)}, bf16[8,40,512]{2,1,0:T(8,128)(2,1)S(1)}, bf16[8,40,512]{2,1,0...) custom-call(s32[2,128]{1,0:T(2,128)} %bitcast.19, ...), custom_call_target="tpu_custom_call" | custom-call | tf_op jit(solution)/shard_map/backward/pallas_call | solution.py:977
  65.8 5.4 %finish.1 = (f32[2048,512]{1,0:T(8,128)}, f32[2048,512]{1,0:T(8,128)}, f32[512,2048]{1,0:T(8,128)}, f32[256,640]{1,0:T(8,128)}, bf16[128,640]{1,0:T(8,128)(2,1)}...) custom-call(bf16[320,2048]{1,0:T(8,128)(2,1)S(1)} %bitcast.12, bf16[320,2048]{1,0:T(8,128)(2,1)S(1)} %bitcast.13, ...), custom_call_target="tpu_custom_call" | custom-call | tf_op jit(solution)/shard_map/finish/pallas_call | solution.py:417
